TPU v7x, 128 devices: a whole 4x4x4 slice. The times are simulated.
128 devices in a mesh: sp: 64 (over z, y, x), tp: 2 (over core).
Axes of the slice: x: 4, y: 4, z: 4, core: 2. Of those that a mesh axis runs over, the one named last changes fastest.
Arguments:
- stream_in: bfloat16 [8192, 2048], P(('sp', 'tp')), may hold values from -6 to 6
- query_rows: bfloat16 [8192, 2048], P('sp', 'tp'), may hold values from -6 to 6
- key_rows: bfloat16 [8192, 2048], P('sp', 'tp'), may hold values from -6 to 6
- value_rows: bfloat16 [8192, 2048], P('sp', 'tp'), may hold values from -6 to 6
- removal_key: bfloat16 [8192, 2048], P('sp', 'tp'), may hold values from -6 to 6
- learn_pre: bfloat16 [8192, 2048], P('sp', 'tp'), may hold values from -12 to 4
- log_rate: float32 [8192, 2048], P('sp', 'tp'), may hold values from -14 to 0
- norm_gain: bfloat16 [2048], P('tp'), may hold values from 0.099609375 to 1.8984375
- out_weight: bfloat16 [2048, 2048], replicated, may hold values from -0.125 to 0.125
- ffn_gain: bfloat16 [2048], replicated, may hold values from 0.099609375 to 1.8984375
- routes: int32 [8192, 2], P(('sp', 'tp')), may hold values from 0 to 31, all different within a row; in each aligned block of 64 rows (0 to 63, 64 to 127, ...) at most 8 rows name the same one
- route_weight: float32 [8192, 2], P(('sp', 'tp')), may hold values from 0.1 to 1
- expert_gate: bfloat16 [64, 2048, 1792], P('sp', None, 'tp'), may hold values from -0.125 to 0.125
- expert_up: bfloat16 [64, 2048, 1792], P('sp', None, 'tp'), may hold values from -0.125 to 0.125
- expert_down: bfloat16 [64, 1792, 2048], P('sp', 'tp'), may hold values from -0.09375 to 0.09375
Outputs:
- layer_out: bfloat16 [8192, 2048], P(('sp', 'tp'))
Inputs may be any that keep to these rules, and one draw needn't show every extreme that they name: `routes`: in each aligned block of 64 rows (the rows of one device after the mixer) no expert is named by more than 8 rows, a bound that some expert reaches in some or all blocks; the experts of one row differ.
All inputs are finite; a program needn't handle non-finite values.
Results may differ from a plain program's by a relative error of at most 0.0065.
Values may be sent and summed in bfloat16 or wider, within the bound.
A program may use at most 192 MiB of HBM per device.

v0:
```python
import jax
import jax.numpy as jnp
from jax import lax
from jax.sharding import Mesh
from jax.sharding import PartitionSpec as P

HEAD = 64
TOPK = 2
SPAN = 16
SP = ("sp_0", "sp_1", "sp_2")
SP_TP = ("sp_0", "sp_1", "sp_2", "tp")


HIGH = lax.Precision.HIGHEST
GROUP_EPS = 0.00064
NORM_EPS = 1e-06
UNIT_EPS = 1e-06


def neutral_like(array, identity):
    return jax.tree.map(
        lambda a, e: jnp.broadcast_to(jnp.asarray(e, a.dtype), a.shape), array, identity
    )


def entering_2(array, axes, combine, identity):
    before = start = neutral_like(array, identity)
    total = array
    for axis in reversed(axes):
        length, place = (lax.axis_size(axis), lax.axis_index(axis))
        pieces = jax.tree.map(lambda part: lax.all_gather(part, axis), total)
        inside, total = (start, start)
        for k in range(length):
            passed = k < place
            total = combine(total, jax.tree.map(lambda part: part[k], pieces))
            inside = jax.tree.map(lambda new, old: jnp.where(passed, new, old), total, inside)
        before = combine(inside, before)
    return before


def from_partner(array, axis, bit):
    return lax.ppermute(array, axis, [(i, i ^ 1 << bit) for i in range(lax.axis_size(axis))])


def split_up(array, dim, length):
    before, after = (array.shape[:dim], array.shape[dim + 1 :])
    return jnp.moveaxis(array.reshape(*before, length, -1, *after), dim, 0)


def sent_and_summed(array, axis, dim):
    length = lax.axis_size(axis)
    pieces = lax.all_to_all(split_up(array, dim, length), axis, 0, 0, tiled=True)
    return jnp.sum(pieces.astype(jnp.float32), axis=0)


def block_terms(queries, key_vals, values, unit_key, pull_key, log_decay):
    span = queries.shape[2]
    head_size = queries.shape[3]
    cumul = jnp.cumsum(log_decay, axis=2)
    before = cumul - log_decay
    position = jnp.arange(span, dtype=jnp.int32)
    strict = (position[:, None] > position[None, :]).astype(jnp.float32)
    upto = (position[:, None] >= position[None, :]).astype(jnp.float32)
    fade_prev = (
        jnp.exp(jnp.minimum(before[:, :, :, None, :] - cumul[:, :, None, :, :], 0.0))
        * strict[:, :, None]
    )
    fade_now = (
        jnp.exp(jnp.minimum(cumul[:, :, :, None, :] - cumul[:, :, None, :, :], 0.0))
        * upto[:, :, None]
    )
    mix_pull = jnp.einsum("bhtk,bhtjk,bhjk->bhtj", unit_key, fade_prev, pull_key, precision=HIGH)
    mix_key = jnp.einsum("bhtk,bhtjk,bhjk->bhtj", unit_key, fade_prev, key_vals, precision=HIGH)
    read_key = jnp.einsum("bhtk,bhtjk,bhjk->bhtj", queries, fade_now, key_vals, precision=HIGH)
    read_pull = jnp.einsum("bhtk,bhtjk,bhjk->bhtj", queries, fade_now, pull_key, precision=HIGH)
    system = mix_pull + jnp.eye(span, dtype=jnp.float32)
    starts = unit_key * jnp.exp(before)
    sources = jnp.concatenate((jnp.matmul(mix_key, values, precision=HIGH), starts), axis=-1)
    solved = lax.linalg.triangular_solve(
        system, sources, left_side=True, lower=True, unit_diagonal=True
    )
    removed = solved[..., :head_size]
    weights = solved[..., head_size:]
    local_read = jnp.matmul(read_key, values, precision=HIGH) - jnp.matmul(
        read_pull, removed, precision=HIGH
    )
    carry_read = queries * jnp.exp(cumul) - jnp.matmul(read_pull, weights, precision=HIGH)
    tail = jnp.exp(cumul[:, :, -1:, :] - cumul)
    key_tail = key_vals * tail
    pull_tail = pull_key * tail
    block_state = jnp.einsum("bhjv,bhjk->bhvk", values, key_tail, precision=HIGH) - jnp.einsum(
        "bhjv,bhjk->bhvk", removed, pull_tail, precision=HIGH
    )
    last_decay = jnp.exp(cumul[:, :, -1, :])
    block_map = last_decay[..., :, None] * jnp.eye(head_size, dtype=jnp.float32) - jnp.einsum(
        "bhjk,bhjl->bhkl", weights, pull_tail, precision=HIGH
    )
    return (block_map, block_state, local_read, carry_read)


def across_blocks(carry, block):
    prefix_map, prefix_state = carry
    block_map, block_state = block
    new_map = jnp.matmul(prefix_map, block_map, precision=HIGH)
    new_state = jnp.matmul(prefix_state, block_map, precision=HIGH) + block_state
    return ((new_map, new_state), (prefix_map, prefix_state))


def compose(earlier, later):
    joined_map = jnp.matmul(earlier[0], later[0], precision=HIGH)
    joined_state = jnp.matmul(earlier[1], later[0], precision=HIGH) + later[1]
    return (joined_map, joined_state)


def local(
    stream_in,
    query_rows,
    key_rows,
    value_rows,
    removal_key,
    learn_pre,
    log_rate,
    norm_gain,
    out_weight,
    ffn_gain,
    routes,
    route_weight,
    expert_gate,
    expert_up,
    expert_down,
):
    tokens_dev = query_rows.shape[0]
    heads_dev = query_rows.shape[1] // HEAD
    blocks = tokens_dev // SPAN

    def blocked(array):
        shaped = array.astype(jnp.float32).reshape(blocks, SPAN, heads_dev, HEAD)
        return shaped.transpose(0, 2, 1, 3)

    removal = blocked(removal_key)
    unit_key = removal / jnp.sqrt(jnp.sum(removal * removal, axis=-1, keepdims=True) + UNIT_EPS)
    pull_key = unit_key * jax.nn.sigmoid(blocked(learn_pre))
    log_decay = -jnp.exp(blocked(log_rate))
    identity = jnp.broadcast_to(jnp.eye(HEAD, dtype=jnp.float32), (heads_dev, HEAD, HEAD))
    nothing = jnp.zeros((heads_dev, HEAD, HEAD), jnp.float32)
    block_map, block_state, local_read, carry_read = block_terms(
        blocked(query_rows), blocked(key_rows), blocked(value_rows), unit_key, pull_key, log_decay
    )
    (device_map, device_state), (prefix_map, prefix_state) = lax.scan(
        across_blocks, (identity, nothing), (block_map, block_state)
    )
    entering = entering_2((device_map, device_state), SP, compose, (identity, nothing))
    block_start = jnp.matmul(entering[1][None], prefix_map, precision=HIGH) + prefix_state
    mixed = local_read + jnp.einsum("bhvk,bhtk->bhtv", block_start, carry_read, precision=HIGH)
    mixed = mixed.transpose(0, 2, 1, 3).reshape(tokens_dev, heads_dev, HEAD)
    centred = mixed - jnp.mean(mixed, axis=-1, keepdims=True)
    variance = jnp.mean(centred * centred, axis=-1, keepdims=True)
    normed = (centred * lax.rsqrt(variance + GROUP_EPS)).reshape(tokens_dev, heads_dev * HEAD)
    normed = (normed * norm_gain.astype(jnp.float32)).astype(jnp.bfloat16)
    gathered = lax.all_to_all(normed, "tp", split_axis=0, concat_axis=1, tiled=True)
    attended = stream_in.astype(jnp.float32) + jnp.dot(
        gathered, out_weight, preferred_element_type=jnp.float32
    )
    scaling = lax.rsqrt(jnp.mean(attended * attended, axis=-1, keepdims=True) + NORM_EPS)
    ffn_in = (attended * scaling * ffn_gain.astype(jnp.float32)).astype(jnp.bfloat16)
    half_rows = attended.shape[0]
    width = attended.shape[1]
    experts = lax.axis_size(SP) // 2
    peers = lax.axis_size(SP) * lax.axis_size("tp")
    capacity = 2 * TOPK * half_rows // experts
    pairs = half_rows * TOPK
    expert_ids = routes.reshape(pairs)
    one_hot = (expert_ids[:, None] == jnp.arange(experts, dtype=jnp.int32)[None, :]).astype(
        jnp.int32
    )
    slot_index = jnp.sum(jnp.cumsum(one_hot, axis=0) * one_hot, axis=1) - 1
    send_index = expert_ids * capacity + slot_index
    send_map = (
        jnp.arange(experts * capacity, dtype=jnp.int32)[:, None] == send_index[None, :]
    ).astype(jnp.bfloat16)
    send_map = jnp.sum(send_map.reshape(experts * capacity, half_rows, TOPK), axis=2)
    dispatched = jnp.dot(send_map, ffn_in, preferred_element_type=jnp.float32).astype(jnp.bfloat16)
    copies = jnp.broadcast_to(
        dispatched.reshape(experts, 1, capacity, width), (experts, 4, capacity, width)
    )
    routed = lax.all_to_all(
        copies.reshape(peers * capacity, width), SP_TP, split_axis=0, concat_axis=0, tiled=True
    )
    gate_act = jnp.dot(routed, expert_gate[0], preferred_element_type=jnp.float32)
    up_act = jnp.dot(routed, expert_up[0], preferred_element_type=jnp.float32)
    hidden = (jax.nn.silu(gate_act) * up_act).astype(jnp.bfloat16)
    partial_out = jnp.dot(hidden, expert_down[0], preferred_element_type=jnp.float32).astype(
        jnp.bfloat16
    )
    partial_out = partial_out.reshape(peers, capacity, width)
    pair_bit = lax.axis_index(SP) % 2
    half_width = width // 2
    kept_half = lax.dynamic_slice_in_dim(partial_out, pair_bit * half_width, half_width, 2)
    sent_half = lax.dynamic_slice_in_dim(partial_out, (1 - pair_bit) * half_width, half_width, 2)
    partner_half = from_partner(sent_half, SP, 0)
    pair_sum = kept_half.astype(jnp.float32) + partner_half.astype(jnp.float32)
    expert_out = sent_and_summed(pair_sum.astype(jnp.bfloat16), "tp", 2).astype(jnp.bfloat16)
    returned = lax.all_to_all(expert_out, SP_TP, split_axis=0, concat_axis=2, tiled=True)
    returned = returned.reshape(capacity * experts, width)
    back_index = slot_index * experts + expert_ids
    back_map = (
        back_index[:, None] == jnp.arange(capacity * experts, dtype=jnp.int32)[None, :]
    ).astype(jnp.bfloat16)
    picked = jnp.dot(back_map, returned, preferred_element_type=jnp.float32).reshape(
        half_rows, TOPK, width
    )
    mixture = jnp.sum(picked * route_weight[:, :, None], axis=1)
    return (attended + mixture).astype(jnp.bfloat16)


def solution(mesh):
    torus = Mesh(mesh.devices.reshape(4, 4, 4, mesh.shape["tp"]), ("sp_0", "sp_1", "sp_2", "tp"))
    return jax.shard_map(
        local,
        mesh=torus,
        in_specs=(
            P(SP_TP, None),
            P(SP, "tp"),
            P(SP, "tp"),
            P(SP, "tp"),
            P(SP, "tp"),
            P(SP, "tp"),
            P(SP, "tp"),
            P("tp"),
            P(),
            P(),
            P(SP_TP, None),
            P(SP_TP, None),
            P(SP, None, "tp"),
            P(SP, None, "tp"),
            P(SP, "tp", None),
        ),
        out_specs=P(SP_TP, None),
        check_vma=False,
    )
```

profile of v0, /device:TPU:1, one launch (start us, length us, event | category | flops | bytes accessed | tf_op | source)
XLA Modules:
  0.0 753.4 jit_solution(138103382372771321)
XLA Ops:
  8.0 5.1 fusion.68
  16.7 2.3 reshape.226
  21.2 2.3 reshape.228
  26.7 4.1 exponential_multiply_fusion.6
  31.2 30.2 %fusion.11 = f32[8,16,16,1,16]{4,3,2,1,0:T(1,128)} fusion(f32[8,16,16,64,1]{3,4,2,1,0:T(1,128)S(1)} %bitcast.186, f32[16,16]{1,0:T(8,128)S(1)} %fusion.173, f32[8,16,16,64]{3,2,1,0:T(8,128)S(1)} %get-tuple-element.130, f32[8,16,16,64]{3,2,1,0:T(8,128)S(1)} %bitcast.193, f32[8,16,16,64]{3,2,1,0:T(8,128)S(1)} %get-tuple-element.134), kind=kOutput, calls=%fused_computation.16 | convolution fusion | flops 33554432 | bytes 2229248 | tf_op jit(solution)/shard_map/bhtk,bhtjk,bhjk->bhtj/dot_general | solution.py:73
  61.5 29.0 %fusion.13 = f32[8,16,16,1,16]{4,3,2,1,0:T(1,128)S(1)} fusion(f32[8,16,16,64,1]{3,4,2,1,0:T(1,128)S(1)} %bitcast.187, f32[16,16]{1,0:T(8,128)S(1)} %fusion.173, f32[8,16,16,64]{3,2,1,0:T(8,128)S(1)} %get-tuple-element.130, f32[8,16,16,64]{3,2,1,0:T(8,128)S(1)} %bitcast_multiply_fusion, f32[8,16,16,64]{3,2,1,0:T(8,128)S(1)} %get-tuple-element.134), kind=kOutput, calls=%fused_computation.18 | convolution fusion | flops 33554432 | bytes 2229248 | tf_op jit(solution)/shard_map/bhtk,bhtjk,bhjk->bhtj/dot_general | solution.py:72
  91.6 160.3 %custom-call.3 = f32[8,16,1,16,16]{3,4,2,1,0:T(8,128)} custom-call(f32[8,16,1,16,16]{4,3,2,1,0:T(8,128)} %add_bitcast_fusion), custom_call_target="InvertDiagBlocksLowerTriangular" | custom-call | tf_op jit(solution)/shard_map/triangular_solve | solution.py:79
  254.0 4.8 fusion.70
  261.0 8.3 %bitcast_subtract_fusion = f32[8,16,64,64]{2,3,1,0:T(8,128)} fusion(f32[8,16,64,64]{3,2,1,0:T(8,128)S(1)} %fusion.70, f32[8,16,16,128]{3,2,1,0:T(8,128)S(1)} %fusion.62, f32[8,16,16,64]{3,2,1,0:T(8,128)S(1)} %bitcast_multiply_fusion, f32[8,16,64]{2,1,0:T(8,128)S(1)} %slice_bitcast_fusion, f32[8,16,16,64]{3,1,2,0:T(8,128)S(1)} %fusion.68), kind=kOutput, calls=%fused_computation.56 | convolution fusion | flops 101449728 | bytes 6324224 | tf_op jit(solution)/shard_map/bhjv,bhjk->bhvk/dot_general | solution.py:91
  269.3 9.7 %multiply_subtract_fusion = f32[8,16,64,64]{3,2,1,0:T(8,128)} fusion(f32[64,64]{1,0:T(8,128)S(1)} %fusion.171, f32[8,16,64]{2,1,0:T(8,128)S(1)} %fusion.186, f32[8,16,16,128]{3,2,1,0:T(8,128)S(1)} %fusion.62, f32[8,16,16,64]{3,2,1,0:T(8,128)S(1)} %bitcast_multiply_fusion, f32[8,16,64]{2,1,0:T(8,128)S(1)} %slice_bitcast_fusion, f32[8,16,16,64]{3,1,2,0:T(8,128)S(1)} %fusion.68), kind=kOutput, calls=%fused_computation.59 | convolution fusion | flops 101974016 | bytes 4276224 | tf_op jit(solution)/shard_map/bhjk,bhjl->bhkl/dot_general | solution.py:95
  279.0 50.6 %while.17 = (s32[]{:T(128)}, f32[16,64,64]{1,2,0:T(8,128)S(1)}, f32[16,64,64]{1,2,0:T(8,128)S(1)}, f32[8,16,64,64]{2,3,1,0:T(8,128)}, f32[8,16,64,64]{3,2,1,0:T(...) while((s32[]{:T(128)}, f32[16,64,64]{1,2,0:T(8,128)S(1)}, ...), condition=%wide.region_3.4_spmd.clone, body=%wide.region_2.3_spmd.clone.sunk | while | flops 100859904 | bytes 6293115 | solution.py:149
  279.2 2.2 fusion.236
  285.5 2.2 fusion.236
  291.8 2.2 fusion.236
  298.2 2.2 fusion.236
  304.5 2.2 fusion.236
  317.1 2.2 fusion.236
  323.4 2.2 fusion.236
  332.9 31.7 %all-gather.13.cloned.1.call-done = f32[64,64,64]{2,1,0:T(8,128)} async-done(((f32[16,64,64]{2,1,0:T(8,128)}), f32[64,64,64]{2,1,0:T(8,128)}) %all-gather.13.cloned.1.call-update) | async-done | bytes 1048592 | tf_op jit(solution)/shard_map/all_gather | solution.py:31
  372.1 2.5 fusion.120
  374.7 18.6 %fusion.17 = f32[8,16,16,1,16]{4,3,2,1,0:T(1,128)} fusion(f32[8,16,16,64]{3,2,1,0:T(8,128)} %bitcast.194, f32[16,16]{1,0:T(8,128)S(1)} %fusion.172, f32[8,16,16,64]{3,2,1,0:T(8,128)S(1)} %copy-done.46, bf16[8,16,16,64,1]{3,2,1,0,4:T(8,128)(2,1)S(1)} %bitcast.198), kind=kOutput, calls=%fused_computation.22 | convolution fusion | flops 33554432 | bytes 1442816 | tf_op jit(solution)/shard_map/bhtk,bhtjk,bhjk->bhtj/dot_general | solution.py:74
  393.3 3.8 all-gather.19.cloned.1.call-done
  405.0 2.7 convolution_add_fusion.8
  407.7 18.1 %fusion.15 = f32[8,16,16,1,16]{4,3,2,1,0:T(1,128)} fusion(f32[8,16,16,64]{3,2,1,0:T(8,128)S(1)} %copy-done.3, f32[16,16]{1,0:T(8,128)S(1)} %fusion.172, f32[8,16,16,64]{3,2,1,0:T(8,128)S(1)} %copy-done.46, bf16[8,16,16,64,1]{3,2,1,0,4:T(8,128)(2,1)} %bitcast.199), kind=kOutput, calls=%fused_computation.20 | convolution fusion | flops 33554432 | bytes 1442816 | tf_op jit(solution)/shard_map/bhtk,bhtjk,bhjk->bhtj/dot_general | solution.py:75
  425.8 3.8 all-gather.15.cloned.1.call-done
  439.3 22.7 %all-gather.21.cloned.1.call-done = f32[64,64,64]{2,1,0:T(8,128)} async-done(((f32[16,64,64]{2,1,0:T(8,128)}), f32[64,64,64]{2,1,0:T(8,128)}) %all-gather.21.cloned.1.call-update) | async-done | bytes 1048592 | tf_op jit(solution)/shard_map/all_gather | solution.py:31
  468.4 2.7 convolution_add_fusion.5
  471.3 3.1 fusion.86
  474.5 3.9 convolution_subtract_fusion
  481.5 13.1 %all-gather.17.cloned.1.call-done = f32[64,64,64]{2,1,0:T(8,128)} async-done(((f32[16,64,64]{2,1,0:T(8,128)}), f32[64,64,64]{2,1,0:T(8,128)}) %all-gather.17.cloned.1.call-update) | async-done | bytes 1048592 | tf_op jit(solution)/shard_map/all_gather | solution.py:31
  494.5 32.4 %all-gather.23.cloned.1.call-done = f32[64,64,64]{2,1,0:T(8,128)} async-done(((f32[16,64,64]{2,1,0:T(8,128)}), f32[64,64,64]{2,1,0:T(8,128)}) %all-gather.23.cloned.1.call-update) | async-done | bytes 1048592 | tf_op jit(solution)/shard_map/all_gather | solution.py:31
  536.1 12.5 %fusion.192 = f32[16,64,8,64]{3,1,0,2:T(8,128)S(1)} fusion(f32[16,64,64,1]{2,1,0,3:T(8,128)S(1)} %fusion.60, f32[8,16,64,64]{2,3,1,0:T(8,128)S(1)} %copy-done.39), kind=kOutput, calls=%fused_computation.253 | convolution fusion | flops 402653184 | bytes 4456448 | tf_op jit(solution)/shard_map/dot_general | solution.py:153
  548.6 6.8 fusion.47
  559.7 4.4 all_to_all.48
  564.2 5.1 multiply_reduce_fusion.1
  569.8 2.5 broadcast_in_dim.58
  572.3 8.7 %all-to-all-start.1 = ((bf16[128,8,2048]{2,1,0:T(8,128)(2,1)}), bf16[128,8,2048]{2,1,0:T(8,128)(2,1)}, u32[]{:S(2)}, u32[]{:S(2)}) async-start(bf16[128,8,2048]{2,1,0:T(8,128)(2,1)} %bitcast.184), calls=%async_computation.1 | async-start | bytes 8388608 | tf_op jit(solution)/shard_map/all_to_all | solution.py:186
  581.0 52.4 %all-to-all-done.1 = bf16[128,8,2048]{2,1,0:T(8,128)(2,1)} async-done(((bf16[128,8,2048]{2,1,0:T(8,128)(2,1)}), bf16[128,8,2048]{2,1,0:T(8,128)(2,1)}, u32[]{:S(2)}, u32[]{:S(2)}) %all-to-all-start.1) | async-done | bytes 4194336 | tf_op jit(solution)/shard_map/all_to_all | solution.py:186
  633.4 7.5 fusion.43
  641.0 7.1 multiply_convert_fusion
  648.1 4.7 convert_bitcast_fusion
  654.6 4.2 copy.235
  658.8 2.9 copy.234
  661.7 43.7 %collective-permute-done = bf16[128,8,1024]{0,2,1:T(8,128)(2,1)} collective-permute-done((bf16[128,8,1024]{0,2,1:T(8,128)(2,1)}, bf16[128,8,1024]{0,2,1:T(8,128)(2,1)}, u32[]{:S(2)}, u32[]{:S(2)}) %collective-permute-start) | collective-permute-done | bytes 2097184 | tf_op jit(solution)/shard_map/ppermute | solution.py:42
  705.4 2.8 add_convert_fusion
  708.1 3.0 copy.211
  711.1 8.0 %all_to_all.49 = bf16[2,128,8,512]{3,2,1,0:T(8,128)(2,1)S(1)} all-to-all(bf16[2,128,8,512]{3,2,1,0:T(8,128)(2,1)} %copy.211), channel_id=1, replica_groups=mesh['sp_0'=4,'sp_1'=4,'sp_2'=4,'tp'=2] {'tp'}, dimensions={0} | all-to-all | bytes 4194304 | tf_op jit(solution)/shard_map/all_to_all | solution.py:52
  720.8 23.4 %all_to_all.50 = bf16[128,8,512]{2,1,0:T(8,128)(2,1)S(1)} all-to-all(bf16[128,8,512]{2,1,0:T(8,128)(2,1)} %reduce_sum.84), channel_id=1, replica_groups=mesh['sp_0'=4,'sp_1'=4,'sp_2'=4,'tp'=2] {'sp_0','sp_1','sp_2','tp'}, dimensions={0} | all-to-all | bytes 2097152 | tf_op jit(solution)/shard_map/all_to_all | solution.py:203
  (271 shorter events, 107.9 us)
Async XLA Ops:
  6.5 358.1 %all-gather.13.cloned.1.call-start = ((), (), s32[]{:S(2)}) async-start(), calls=%async_computation.4 | async-start | bytes 2621440 | tf_op jit(solution)/shard_map/all_gather | solution.py:31
  14.6 239.3 %copy-start.5 = (bf16[8,16,16,64]{3,2,1,0:T(8,128)(2,1)}, bf16[8,16,16,64]{3,2,1,0:T(8,128)(2,1)S(1)}, u32[]{:S(2)}) copy-start(bf16[8,16,16,64]{3,2,1,0:T(8,128)(2,1)S(1)} %reshape.219) | copy-start | bytes 786436
  30.8 30.6 %copy-start.45 = (f32[8,16,16,64]{3,2,1,0:T(8,128)}, f32[8,16,16,64]{3,2,1,0:T(8,128)S(1)}, u32[]{:S(2)}) copy-start(f32[8,16,16,64]{3,2,1,0:T(8,128)S(1)} %get-tuple-element.134) | copy-start | bytes 1572868
  31.2 238.1 %copy-start.2 = (f32[8,16,16,64]{3,2,1,0:T(8,128)}, f32[8,16,16,64]{3,2,1,0:T(8,128)S(1)}, u32[]{:S(2)}) copy-start(f32[8,16,16,64]{3,2,1,0:T(8,128)S(1)} %bitcast_multiply_fusion) | copy-start | bytes 1572868
  251.9 6.9 copy-start.41
  251.9 6.9 copy-start.48
  261.0 8.3 %copy-start = (f32[8,16,16,128]{3,2,1,0:T(8,128)}, f32[8,16,16,128]{3,2,1,0:T(8,128)S(1)}, u32[]{:S(2)}) copy-start(f32[8,16,16,128]{3,2,1,0:T(8,128)S(1)} %fusion.62) | copy-start | bytes 3145732
  279.0 52.8 %copy-start.53 = (s32[64,2]{0,1:T(2,128)S(1)}, s32[64,2]{0,1:T(2,128)}, u32[]{:S(2)}) copy-start(s32[64,2]{0,1:T(2,128)} %param.27) | copy-start | bytes 1540
  279.0 53.4 %copy-start.51 = (bf16[128,1024]{1,0:T(8,128)(2,1)S(1)}, bf16[128,1024]{1,0:T(8,128)(2,1)}, u32[]{:S(2)}) copy-start(bf16[128,1024]{1,0:T(8,128)(2,1)} %param.18) | copy-start | bytes 786436
  330.7 66.4 %all-gather.19.cloned.1.call-start = ((), (), s32[]{:S(2)}) async-start(), calls=%async_computation.7 | async-start | bytes 2621440 | tf_op jit(solution)/shard_map/all_gather | solution.py:31
  331.8 97.8 %all-gather.15.cloned.1.call-start = ((), (), s32[]{:S(2)}) async-start(), calls=%async_computation.5 | async-start | bytes 2621440 | tf_op jit(solution)/shard_map/all_gather | solution.py:31
  332.0 42.7 %copy-start.46 = (f32[8,16,16,64]{3,2,1,0:T(8,128)S(1)}, f32[8,16,16,64]{3,2,1,0:T(8,128)}, u32[]{:S(2)}) copy-start(f32[8,16,16,64]{3,2,1,0:T(8,128)} %copy-done.45) | copy-start | bytes 1572868
  332.7 42.0 %copy-start.9 = (bf16[8,16,16,64]{3,2,1,0:T(8,128)(2,1)}, bf16[8,16,16,64]{3,2,1,0:T(8,128)(2,1)S(1)}, u32[]{:S(2)}) copy-start(bf16[8,16,16,64]{3,2,1,0:T(8,128)(2,1)S(1)} %reshape.218) | copy-start | bytes 786436
  332.9 41.8 %copy-start.49 = (bf16[8,16,16,64]{3,1,2,0:T(8,128)(2,1)}, bf16[8,16,16,64]{3,1,2,0:T(8,128)(2,1)S(1)}, u32[]{:S(2)}) copy-start(bf16[8,16,16,64]{3,1,2,0:T(8,128)(2,1)S(1)} %copy.289) | copy-start | bytes 786436
  374.6 87.3 %all-gather.21.cloned.1.call-start = ((), (), s32[]{:S(2)}) async-start(), calls=%async_computation.8 | async-start | bytes 2621440 | tf_op jit(solution)/shard_map/all_gather | solution.py:31
  393.3 14.4 %copy-start.3 = (f32[8,16,16,64]{3,2,1,0:T(8,128)S(1)}, f32[8,16,16,64]{3,2,1,0:T(8,128)}, u32[]{:S(2)}) copy-start(f32[8,16,16,64]{3,2,1,0:T(8,128)} %copy-done.2) | copy-start | bytes 1572868
  407.6 86.9 %all-gather.17.cloned.1.call-start = ((), (), s32[]{:S(2)}) async-start(), calls=%async_computation.6 | async-start | bytes 2621440 | tf_op jit(solution)/shard_map/all_gather | solution.py:31
  429.6 7.5 copy-start.4
  438.6 88.3 %all-gather.23.cloned.1.call-start = ((), (), s32[]{:S(2)}) async-start(), calls=%async_computation.9 | async-start | bytes 2621440 | tf_op jit(solution)/shard_map/all_gather | solution.py:31
  439.3 31.9 %copy-start.54 = (bf16[1024]{0:T(1024)(128)(2,1)S(1)}, bf16[1024]{0:T(1024)(128)(2,1)}, u32[]{:S(2)}) copy-start(bf16[1024]{0:T(1024)(128)(2,1)} %param.24) | copy-start | bytes 6148
  439.3 32.0 %copy-start.52 = (bf16[2048]{0:T(1024)(128)(2,1)S(1)}, bf16[2048]{0:T(1024)(128)(2,1)}, u32[]{:S(2)}) copy-start(bf16[2048]{0:T(1024)(128)(2,1)} %param.26) | copy-start | bytes 12292
  465.5 5.8 copy-start.6
  465.5 8.9 %copy-start.1 = (f32[8,16,16,128]{3,2,1,0:T(8,128)S(1)}, f32[8,16,16,128]{3,2,1,0:T(8,128)}, u32[]{:S(2)}) copy-start(f32[8,16,16,128]{3,2,1,0:T(8,128)} %copy-done) | copy-start | bytes 3145732
  465.5 8.9 %copy-start.10 = (bf16[8,16,16,64]{3,2,1,0:T(8,128)(2,1)S(1)}, bf16[8,16,16,64]{3,2,1,0:T(8,128)(2,1)}, u32[]{:S(2)}) copy-start(bf16[8,16,16,64]{3,2,1,0:T(8,128)(2,1)} %copy-done.9) | copy-start | bytes 786436
  471.2 7.1 copy-start.12
  471.2 7.1 copy-start.14
  471.2 7.1 copy-start.21
  471.3 7.1 copy-start.22
  474.4 4.7 copy-start.36
  474.4 6.3 copy-start.16
  474.4 6.3 copy-start.18
  474.4 6.3 copy-start.23
  474.4 6.2 copy-start.25
  528.7 6.6 copy-start.8
  528.7 6.6 copy-start.19
  528.7 6.6 copy-start.27
  528.7 6.6 copy-start.29
  528.7 6.6 copy-start.44
  536.1 12.5 %copy-start.38 = (f32[8,16,64,64]{3,2,1,0:T(8,128)S(1)}, f32[8,16,64,64]{3,2,1,0:T(8,128)}, u32[]{:S(2)}) copy-start(f32[8,16,64,64]{3,2,1,0:T(8,128)} %get-tuple-element.48) | copy-start | bytes 6291460
  536.1 12.5 %copy-start.40 = (f32[8,16,16,64]{3,2,1,0:T(8,128)S(1)}, f32[8,16,16,64]{3,2,1,0:T(8,128)}, u32[]{:S(2)}) copy-start(f32[8,16,16,64]{3,2,1,0:T(8,128)} %convolution_subtract_fusion) | copy-start | bytes 1572868
  548.6 6.8 copy-start.42
  548.6 6.8 copy-start.43
  558.2 6.0 copy-start.50
  572.3 61.1 %all-to-all-start.1 = ((bf16[128,8,2048]{2,1,0:T(8,128)(2,1)}), bf16[128,8,2048]{2,1,0:T(8,128)(2,1)}, u32[]{:S(2)}, u32[]{:S(2)}) async-start(bf16[128,8,2048]{2,1,0:T(8,128)(2,1)} %bitcast.184), calls=%async_computation.1 | async-start | bytes 8388608 | tf_op jit(solution)/shard_map/all_to_all | solution.py:186
  633.4 7.5 copy-start.56
  641.0 7.1 copy-start.57
  658.8 46.6 %collective-permute-start = (bf16[128,8,1024]{0,2,1:T(8,128)(2,1)}, bf16[128,8,1024]{0,2,1:T(8,128)(2,1)}, u32[]{:S(2)}, u32[]{:S(2)}) collective-permute-start(bf16[128,8,1024]{0,2,1:T(8,128)(2,1)} %copy.235), channel_id=1, source_target_pairs={{0,2},{2,0},{4,6},{6,4},{8,10},{10,8},{12,14},{14,12},{16,18},{18,... | collective-permute-start | bytes 6291464 | tf_op jit(solution)/shard_map/ppermute | solution.py:42
  719.1 26.1 %copy-start.55 = (f32[64,2]{0,1:T(2,128)S(1)}, f32[64,2]{0,1:T(2,128)}, u32[]{:S(2)}) copy-start(f32[64,2]{0,1:T(2,128)} %param.28) | copy-start | bytes 1540
  (18 other events, 38.2 us)
Sparse Core Ops, SparseCore 0:
  330.8 33.7 all-gather.12
  366.3 30.7 all-gather.18
  398.8 30.8 all-gather.14
  431.2 30.7 all-gather.20
  463.5 31.0 all-gather.16
  496.1 30.8 all-gather.22
where the time goes:
time: 759 us; the launch traced here: 753 us
  matrix products  252 us (33%)
  waiting for transfers between devices  204 us (27%)
  other arithmetic  183 us (24%)
  local copies, waits for them, and re-layouts  54.5 us (7%)
  blocking collectives  35.8 us (5%)
  between operations  14.9 us (2%)
  starting transfers between devices  9.12 us (1%)
    another operation x5, other arithmetic, block_terms(): lax.linalg.triangular_solve(system, sources, left_side=True, lower=True,...  161 us
    all_gather x6, waiting for transfers between devices, entering_2(): pieces = jax.tree.map(lambda part: lax.all_gather(part, axis), total)  107 us
    all_to_all x1, waiting for transfers between devices, local(): lax.all_to_all(copies.reshape(peers * capacity, width), SP_TP, split_axis...  52.4 us
    ppermute x1, waiting for transfers between devices, from_partner(): lax.ppermute(array, axis, [(i, i ^ 1 << bit) for i in range(lax.axis_size...  43.7 us
    dot_general x1, matrix products, block_terms(): jnp.einsum('bhtk,bhtjk,bhjk->bhtj', unit_key, fade_prev, key_vals, precis...  30.2 us
    dot_general x1, matrix products, block_terms(): jnp.einsum('bhtk,bhtjk,bhjk->bhtj', unit_key, fade_prev, pull_key, precis...  29 us
    dot_general x15, matrix products, compose(): joined_state = jnp.matmul(earlier[1], later[0], precision=HIGH) + later[1]  26.8 us
    all_to_all x1, blocking collectives, local(): lax.all_to_all(expert_out, SP_TP, split_axis=0, concat_axis=2, tiled=True)  23.4 us
  transfers between devices with their start and end apart: 8, of which 8 were waited for; matrix products, arithmetic and copies ran while one was open for 11% of the time, Pallas kernels for 0%

commit v1 on v0

v1 whole, which is shorter than its diff:
```python
import functools
from typing import NamedTuple

import jax
import jax.numpy as jnp
from jax import lax
from jax.experimental import pallas as pl
from jax.experimental.pallas import tpu as pltpu
from jax.sharding import Mesh
from jax.sharding import PartitionSpec as P

HEAD = 64
LANES = 128
F32 = jnp.float32
BF16 = jnp.bfloat16
UNIT_EPS = 1e-06


def split(x):
    high = x.astype(BF16)
    return high, (x - high.astype(F32)).astype(BF16)


def mxu(x, y, dims=((1,), (0,))):
    return lax.dot_general(x, y, (dims, ((), ())), preferred_element_type=F32)


def packed(x):
    return jnp.concatenate(x, axis=1)


def spread(y):
    high, low = y
    top = jnp.concatenate((high, low), axis=1)
    return jnp.concatenate((top, top), axis=0)


def folded(z):
    half = z.shape[1] // 2
    return z[:, :half] + z[:, half:]


def product(x, y):
    return folded(mxu(packed(x), spread(y)))


def iota(shape, dim):
    return lax.broadcasted_iota(jnp.int32, shape, dim)


class Masks(NamedTuple):
    same_head: jax.Array
    lower: jax.Array


class Prepared(NamedTuple):
    left: list
    right: list
    values: jax.Array
    starts: jax.Array
    query_now: jax.Array
    pull_tail: jax.Array
    key_tail: jax.Array
    decay_all: jax.Array


def mixer_prepare(refs, lanes, masks):
    q_ref, k_ref, v_ref, r_ref, l_ref, g_ref = refs
    tokens = q_ref.shape[0]
    removal = r_ref[:, lanes].astype(F32)
    squares = split(removal * removal)
    total = mxu(packed(squares), jnp.concatenate((masks.same_head, masks.same_head), axis=0))
    unit = removal * lax.rsqrt(total + UNIT_EPS)
    pull = unit * jax.nn.sigmoid(l_ref[:, lanes].astype(F32))
    log_decay = -jnp.exp(g_ref[:, lanes])
    high = log_decay.astype(BF16)
    rest = log_decay - high.astype(F32)
    mid = rest.astype(BF16)
    low = (rest - mid.astype(F32)).astype(BF16)
    stacked = jnp.concatenate((packed((high, mid)), packed((low, jnp.zeros_like(low)))), axis=0)
    cumul = folded(mxu(packed((masks.lower, masks.lower)), stacked))
    middle = cumul[tokens // 2 - 1 : tokens // 2]
    end = cumul[tokens - 1 : tokens]
    grown = jnp.exp(middle - cumul)
    faded = jnp.exp(cumul - middle)
    unit_hat = unit * jnp.exp(cumul - log_decay - middle)
    query_hat = q_ref[:, lanes].astype(F32) * faded
    pull_hat = pull * grown
    key_hat = k_ref[:, lanes].astype(F32) * grown
    from_start = jnp.exp(middle)
    to_end = jnp.exp(end - middle)
    values = v_ref[:, lanes]
    left = [jnp.concatenate(p, axis=0) for p in zip(split(unit_hat), split(query_hat))]
    right = [jnp.concatenate(p, axis=0) for p in zip(split(pull_hat), split(key_hat))]
    return Prepared(
        left,
        right,
        jnp.concatenate((values, values), axis=0),
        pltpu.roll(unit_hat * from_start, HEAD, 1),
        query_hat * from_start,
        spread(split(pull_hat * to_end)),
        jnp.concatenate(split(key_hat * to_end), axis=0),
        jnp.exp(end),
    )


def mixer_kernel(pairs, q_ref, k_ref, v_ref, r_ref, l_ref, g_ref, z_ref, local_ref, carry_ref):
    refs = (q_ref, k_ref, v_ref, r_ref, l_ref, g_ref)
    tokens = q_ref.shape[0]
    row, col = iota((tokens, tokens), 0), iota((tokens, tokens), 1)
    strict, upto, apart = row > col, row >= col, row ^ col
    first = iota((tokens, LANES), 1) < HEAD
    masks = Masks(
        ((iota((LANES, LANES), 0) < HEAD) == (iota((LANES, LANES), 1) < HEAD)).astype(BF16),
        upto.astype(BF16),
    )
    own_lanes = (first, jnp.logical_not(first))
    lanes = [slice(pair * LANES, (pair + 1) * LANES) for pair in range(pairs)]
    ready = [mixer_prepare(refs, part, masks) for part in lanes]
    heads = [(pair, head) for pair in range(pairs) for head in range(2)]

    scores = []
    for pair, head in heads:
        inside = jnp.concatenate((own_lanes[head], own_lanes[head]), axis=0)
        own = [jnp.where(inside, x, jnp.zeros_like(x)) for x in ready[pair].left]
        right = ready[pair].right
        scores.append(
            mxu(packed(own), packed((right[0], right[0])), ((1,), (1,)))
            + mxu(own[0], right[1], ((1,), (1,)))
        )
    mix_pull = [jnp.where(strict, s[:tokens, :tokens], 0.0) for s in scores]
    mix_key = [jnp.where(strict, s[:tokens, tokens:], 0.0) for s in scores]
    read_pull = [split(jnp.where(upto, s[tokens:, :tokens], 0.0)) for s in scores]
    read_key = [jnp.where(upto, s[tokens:, tokens:], 0.0) for s in scores]
    by_key = []
    for n, (pair, head) in enumerate(heads):
        both = [jnp.concatenate(p, axis=0) for p in zip(split(mix_key[n]), split(read_key[n]))]
        by_key.append(mxu(packed(both), ready[pair].values))

    identity = (row == col).astype(F32)
    inverse = [identity - jnp.where(apart < 2, m, 0.0) for m in mix_pull]
    size = 2
    while size < tokens:
        within = (apart >= size) & (apart < 2 * size)
        parts = [split(x) for x in inverse]
        edges = [split(jnp.where(within, m, 0.0)) for m in mix_pull]
        steps = [split(product(x, y)) for x, y in zip(parts, edges)]
        inverse = [x - product(y, z) for x, y, z in zip(inverse, steps, parts)]
        size *= 2

    answers, solved, outer = [], [], []
    for n, (pair, head) in enumerate(heads):
        sources = jnp.where(own_lanes[head], by_key[n][:tokens], ready[pair].starts)
        answers.append(split(product(split(inverse[n]), split(sources))))
    for n, (pair, head) in enumerate(heads):
        solved.append(product(read_pull[n], answers[n]))
        stacked = jnp.concatenate(answers[n], axis=0)
        outer.append(folded(mxu(stacked, ready[pair].pull_tail, ((0,), (0,)))))

    half = iota((HEAD, LANES), 1) < HEAD
    diagonal = (iota((HEAD, LANES), 1) % HEAD) == iota((HEAD, LANES), 0)
    for pair in range(pairs):
        one, two = 2 * pair, 2 * pair + 1
        local_ref[:, lanes[pair]] = jnp.where(
            first, by_key[one][tokens:] - solved[one], by_key[two][tokens:] - solved[two]
        )
        carry_ref[:, lanes[pair]] = ready[pair].query_now - pltpu.roll(
            jnp.where(first, solved[two], solved[one]), HEAD, 1
        )
        written = mxu(ready[pair].values, ready[pair].key_tail, ((0,), (0,)))
        z_ref[pair, :HEAD] = jnp.where(
            half, written[:HEAD] - outer[one][:HEAD], written[HEAD:] - outer[two][HEAD:]
        )
        z_ref[pair, HEAD:] = jnp.where(diagonal, ready[pair].decay_all, 0.0) - jnp.where(
            half, outer[one][HEAD:], outer[two][:HEAD]
        )


def mixer_blocks(queries, keys, values, removal, learn, rates, per_step=2):
    tokens, width = queries.shape
    pairs = width // LANES
    rows = pl.BlockSpec((tokens, per_step * LANES), lambda i: (0, i))
    return pl.pallas_call(
        functools.partial(mixer_kernel, per_step),
        grid=(pairs // per_step,),
        in_specs=[rows] * 6,
        out_specs=[pl.BlockSpec((per_step, 2 * HEAD, LANES), lambda i: (i, 0, 0)), rows, rows],
        out_shape=[
            jax.ShapeDtypeStruct((pairs, 2 * HEAD, LANES), F32),
            jax.ShapeDtypeStruct((tokens, width), F32),
            jax.ShapeDtypeStruct((tokens, width), F32),
        ],
        name="mixer_blocks",
    )(queries, keys, values, removal, learn, rates)


MESH = pl.DeviceIdType.MESH
GROUP_EPS = 0.00064
NORM_EPS = 1e-06
COLUMNS = 512


def block_diagonal(rows):
    first = iota(rows.shape, 1) < HEAD
    zero = jnp.zeros_like(rows)
    return jnp.concatenate((jnp.where(first, rows, zero), jnp.where(first, zero, rows)), axis=0)


def mapped(earlier, later):
    return product(split(earlier), split(block_diagonal(later[HEAD:])))


def compose(earlier, later):
    joined = mapped(earlier, later)
    return jnp.concatenate((joined[:HEAD] + later[:HEAD], joined[HEAD:]), axis=0)


def prefixes(blocks):
    done, step = list(blocks), 1
    while step < len(done):
        for j in range(len(done)):
            if (j // step) % 2 == 1:
                done[j] = compose(done[j // step * step - 1], done[j])
        step *= 2
    return done


def joined_all(blocks):
    while len(blocks) > 1:
        pairs = [compose(*blocks[j : j + 2]) for j in range(0, len(blocks) - 1, 2)]
        blocks = pairs + (blocks[-1:] if len(blocks) % 2 else [])
    return blocks[0]


def remote(source, target, sends, receives, place):
    return pltpu.make_async_remote_copy(
        src_ref=source,
        dst_ref=target,
        send_sem=sends,
        recv_sem=receives,
        device_id=place,
        device_id_type=MESH,
    )


def entering_states(z_ref, by_member, by_group, total_ref, found, entered, sems):
    group, member, core = (lax.axis_index(a) for a in ("grp", "mem", "tp"))
    members, groups = by_member.shape[0], by_group.shape[0]
    sent_1, got_1, sent_2, got_2, sent_3, got_3 = sems

    first = []
    for offset in range(1, members):
        peer = lax.rem(member + offset, members)
        copy = remote(
            z_ref.at[peer],
            by_member.at[member],
            sent_1.at[offset],
            got_1.at[member],
            (group, peer, core),
        )
        copy.start()
        first.append(copy)
    by_member[member] = z_ref[member]
    for offset in range(1, members):
        peer = lax.rem(member + offset, members)
        remote(
            z_ref.at[peer], by_member.at[peer], sent_1.at[offset], got_1.at[peer], (group, peer, core)
        ).wait_recv()
    inclusive = prefixes([by_member[j] for j in range(members)])
    total_ref[...] = inclusive[-1]

    second = []
    for offset in range(1, groups):
        peer = lax.rem(group + offset, groups)
        copy = remote(
            total_ref,
            by_group.at[group],
            sent_2.at[offset],
            got_2.at[group],
            (peer, member, core),
        )
        copy.start()
        second.append(copy)
    maps = [spread(split(block_diagonal(inclusive[j][HEAD:]))) for j in range(members - 1)]
    by_group[group] = total_ref[...]
    for offset in range(1, groups):
        peer = lax.rem(group + offset, groups)
        remote(
            total_ref, by_group.at[peer], sent_2.at[offset], got_2.at[peer], (peer, member, core)
        ).wait_recv()
    shape = total_ref.shape
    neutral = ((iota(shape, 1) % HEAD) + HEAD == iota(shape, 0)).astype(F32)
    before = [jnp.where(j < group, by_group[j], neutral) for j in range(groups - 1)]
    start = joined_all(before)[:HEAD]
    parts = packed(split(start))
    found[0] = start
    for j in range(1, members):
        found[j] = folded(mxu(parts, maps[j - 1])) + inclusive[j - 1][:HEAD]

    third = []
    for offset in range(1, members):
        peer = lax.rem(member + offset, members)
        copy = remote(
            found.at[peer],
            entered.at[member],
            sent_3.at[offset],
            got_3.at[member],
            (group, peer, core),
        )
        copy.start()
        third.append(copy)
    entered[member] = found[member]
    for offset in range(1, members):
        peer = lax.rem(member + offset, members)
        remote(
            found.at[peer], entered.at[peer], sent_3.at[offset], got_3.at[peer], (group, peer, core)
        ).wait_recv()
    return first + second + third


def normed_heads(local_ref, carry_ref, entered, gain_ref, normed):
    same_head = ((iota((LANES, LANES), 0) < HEAD) == (iota((LANES, LANES), 1) < HEAD)).astype(BF16)
    same_head = jnp.concatenate((same_head, same_head), axis=0)
    pairs = entered.shape[0]
    lanes = [slice(pair * LANES, (pair + 1) * LANES) for pair in range(pairs)]
    mixed = []
    for pair in range(pairs):
        high, low = split(block_diagonal(entered[pair]))
        rhs = jnp.concatenate((packed((high, high)), packed((low, low))), axis=0)
        read = folded(mxu(packed(split(carry_ref[:, lanes[pair]])), rhs, ((1,), (1,))))
        mixed.append(local_ref[:, lanes[pair]] + read)
    centred = [x - mxu(packed(split(x)), same_head) * (1.0 / HEAD) for x in mixed]
    variance = [mxu(packed(split(x * x)), same_head) * (1.0 / HEAD) for x in centred]
    for pair in range(pairs):
        scaled = centred[pair] * lax.rsqrt(variance[pair] + GROUP_EPS)
        normed[:, lanes[pair]] = (scaled * gain_ref[:, lanes[pair]].astype(F32)).astype(BF16)


def slot_map(routes_ref, experts, capacity):
    half = routes_ref.shape[0]
    shape = (half, experts * capacity)
    lane = iota(shape, 1)
    expert, slot = lane // capacity, lane % capacity
    named = [routes_ref[:, k : k + 1] == expert for k in range(2)]
    chosen = (named[0] | named[1]).astype(F32)
    earlier = (iota((half, half), 0) > iota((half, half), 1)).astype(BF16)
    place = mxu(earlier, chosen.astype(BF16))
    kept = jnp.where(place == slot.astype(F32), chosen, 0.0)
    return kept, named


def mixer_finish_kernel(
    experts,
    z_ref,
    local_ref,
    carry_ref,
    gain_ref,
    stream_ref,
    weight_ref,
    ffn_gain_ref,
    routes_ref,
    attended_ref,
    dispatched_ref,
    by_member,
    by_group,
    total_ref,
    found,
    entered,
    normed,
    weight,
    partial,
    other,
    weight_sem,
    sent_4,
    got_4,
    *sems,
):
    group, member, core = (lax.axis_index(a) for a in ("grp", "mem", "tp"))
    members, groups = by_member.shape[0], by_group.shape[0]
    barrier = pltpu.get_barrier_semaphore()
    peers = [(group, lax.rem(member + o, members), core) for o in range(1, members)]
    peers += [(lax.rem(group + o, groups), member, core) for o in range(1, groups)]
    peers += [(group, member, 1 - core)]
    for peer in peers:
        pl.semaphore_signal(barrier, inc=1, device_id=peer, device_id_type=MESH)
    depth = weight.shape[0]
    fetch = pltpu.make_async_copy(weight_ref.at[pl.ds(core * depth, depth)], weight, weight_sem)
    fetch.start()
    pl.semaphore_wait(barrier, len(peers))

    copies = entering_states(z_ref, by_member, by_group, total_ref, found, entered, sems)
    normed_heads(local_ref, carry_ref, entered, gain_ref, normed)
    fetch.wait()
    half = stream_ref.shape[0]
    chunks = partial.shape[0]
    mine, theirs = pl.ds(core * half, half), pl.ds((1 - core) * half, half)
    for n in range(chunks):
        partial[n] = jnp.dot(
            normed[...], weight[:, n * COLUMNS : (n + 1) * COLUMNS], preferred_element_type=F32
        )
        copy = remote(
            partial.at[n, theirs],
            other.at[n],
            sent_4.at[n],
            got_4.at[n],
            (group, member, 1 - core),
        )
        copy.start()
        copies.append(copy)
    kept, _ = slot_map(routes_ref, experts, dispatched_ref.shape[0] // experts)
    kept = kept.astype(BF16)
    squares = jnp.zeros((half, 1), F32)
    for n in range(chunks):
        lanes = slice(n * COLUMNS, (n + 1) * COLUMNS)
        copies[n - chunks].wait_recv()
        attended = stream_ref[:, lanes].astype(F32) + (partial[n, mine] + other[n])
        attended_ref[:, lanes] = attended
        squares = squares + jnp.sum(attended * attended, axis=1, keepdims=True)
    width = chunks * COLUMNS
    scaling = lax.rsqrt(squares * (1.0 / width) + NORM_EPS)
    for n in range(chunks):
        lanes = slice(n * COLUMNS, (n + 1) * COLUMNS)
        ffn_in = attended_ref[:, lanes] * scaling * ffn_gain_ref[:, lanes].astype(F32)
        dispatched_ref[:, lanes] = mxu(kept, ffn_in.astype(BF16), ((0,), (0,))).astype(BF16)
    for copy in copies:
        copy.wait_send()


def mixer_finish(z, local_read, carry_read, gain, stream, weight, ffn_gain, routes, experts, capacity):
    half, width = stream.shape
    tokens = local_read.shape[0]
    members, groups = lax.axis_size("mem"), lax.axis_size("grp")
    chunks = width // COLUMNS
    vmem = pl.BlockSpec(memory_space=pltpu.VMEM)
    dma = pltpu.SemaphoreType.DMA
    return pl.pallas_call(
        functools.partial(mixer_finish_kernel, experts),
        in_specs=[vmem] * 5 + [pl.BlockSpec(memory_space=pl.ANY)] + [vmem] * 2,
        out_specs=[vmem, vmem],
        out_shape=[
            jax.ShapeDtypeStruct((half, width), F32),
            jax.ShapeDtypeStruct((experts * capacity, width), BF16),
        ],
        scratch_shapes=[
            pltpu.VMEM((members, 2 * HEAD, LANES), F32),
            pltpu.VMEM((groups, 2 * HEAD, LANES), F32),
            pltpu.VMEM((2 * HEAD, LANES), F32),
            pltpu.VMEM((members, HEAD, LANES), F32),
            pltpu.VMEM((members, HEAD, LANES), F32),
            pltpu.VMEM((tokens, width // 2), BF16),
            pltpu.VMEM((width // 2, width), BF16),
            pltpu.VMEM((chunks, tokens, COLUMNS), F32),
            pltpu.VMEM((chunks, half, COLUMNS), F32),
            dma,
            dma((chunks,)),
            dma((chunks,)),
            dma((members,)),
            dma((members,)),
            dma((groups,)),
            dma((groups,)),
            dma((members,)),
            dma((members,)),
        ],
        compiler_params=pltpu.CompilerParams(
            collective_id=0, has_side_effects=True, vmem_limit_bytes=48 * 1024 * 1024
        ),
        name="mixer_finish",
    )(z, local_read, carry_read, gain, stream, weight, ffn_gain, routes)


TOPK = 2
SP_TP = ("grp", "mem", "tp")
SP = ("grp", "mem")


def from_partner(array, axis, bit):
    return lax.ppermute(array, axis, [(i, i ^ 1 << bit) for i in range(lax.axis_size(axis))])


def split_up(array, dim, length):
    before, after = (array.shape[:dim], array.shape[dim + 1 :])
    return jnp.moveaxis(array.reshape(*before, length, -1, *after), dim, 0)


def sent_and_summed(array, axis, dim):
    length = lax.axis_size(axis)
    pieces = lax.all_to_all(split_up(array, dim, length), axis, 0, 0, tiled=True)
    return jnp.sum(pieces.astype(jnp.float32), axis=0)


def local(
    stream_in,
    query_rows,
    key_rows,
    value_rows,
    removal_key,
    learn_pre,
    log_rate,
    norm_gain,
    out_weight,
    ffn_gain,
    routes,
    route_weight,
    expert_gate,
    expert_up,
    expert_down,
):
    half_rows, width = stream_in.shape
    experts = lax.axis_size(SP) // 2
    peers = lax.axis_size(SP_TP)
    capacity = 2 * TOPK * half_rows // experts
    z, local_read, carry_read = mixer_blocks(
        query_rows, key_rows, value_rows, removal_key, learn_pre, log_rate, per_step=4
    )
    attended, dispatched = mixer_finish(
        z,
        local_read,
        carry_read,
        norm_gain.reshape(1, -1),
        stream_in,
        out_weight,
        ffn_gain.reshape(1, -1),
        routes,
        experts,
        capacity,
    )
    copies = jnp.broadcast_to(
        dispatched.reshape(experts, 1, capacity, width), (experts, 4, capacity, width)
    )
    routed = lax.all_to_all(
        copies.reshape(peers * capacity, width), SP_TP, split_axis=0, concat_axis=0, tiled=True
    )
    gate_act = jnp.dot(routed, expert_gate[0], preferred_element_type=jnp.float32)
    up_act = jnp.dot(routed, expert_up[0], preferred_element_type=jnp.float32)
    hidden = (jax.nn.silu(gate_act) * up_act).astype(jnp.bfloat16)
    partial_out = jnp.dot(hidden, expert_down[0], preferred_element_type=jnp.float32).astype(
        jnp.bfloat16
    )
    partial_out = partial_out.reshape(peers, capacity, width)
    pair_bit = lax.axis_index(SP) % 2
    half_width = width // 2
    kept_half = lax.dynamic_slice_in_dim(partial_out, pair_bit * half_width, half_width, 2)
    sent_half = lax.dynamic_slice_in_dim(partial_out, (1 - pair_bit) * half_width, half_width, 2)
    partner_half = from_partner(sent_half, SP, 0)
    pair_sum = kept_half.astype(jnp.float32) + partner_half.astype(jnp.float32)
    expert_out = sent_and_summed(pair_sum.astype(jnp.bfloat16), "tp", 2).astype(jnp.bfloat16)
    returned = lax.all_to_all(expert_out, SP_TP, split_axis=0, concat_axis=2, tiled=True)
    returned = returned.reshape(capacity, experts, width)
    lane = jnp.arange(experts, dtype=jnp.int32)
    one_hot = (routes[:, :, None] == lane).any(axis=1)
    earlier = jnp.arange(half_rows)[:, None] > jnp.arange(half_rows)[None, :]
    place = jnp.dot(earlier.astype(jnp.float32), one_hot.astype(jnp.float32))
    slot = jnp.take_along_axis(place.astype(jnp.int32), routes, axis=1).reshape(-1)
    back_index = slot * experts + routes.reshape(-1)
    back_map = (
        back_index[:, None] == jnp.arange(capacity * experts, dtype=jnp.int32)[None, :]
    ).astype(jnp.bfloat16)
    picked = jnp.dot(
        back_map, returned.reshape(capacity * experts, width), preferred_element_type=jnp.float32
    ).reshape(half_rows, TOPK, width)
    mixture = jnp.sum(picked * route_weight[:, :, None], axis=1)
    return (attended + mixture).astype(jnp.bfloat16)


def solution(mesh):
    sp = mesh.shape["sp"]
    groups = 1
    while groups * groups < sp:
        groups *= 2
    torus = Mesh(
        mesh.devices.reshape(sp // groups, groups, mesh.shape["tp"]), ("grp", "mem", "tp")
    )
    return jax.shard_map(
        local,
        mesh=torus,
        in_specs=(
            P(SP_TP, None),
            P(SP, "tp"),
            P(SP, "tp"),
            P(SP, "tp"),
            P(SP, "tp"),
            P(SP, "tp"),
            P(SP, "tp"),
            P("tp"),
            P(),
            P(),
            P(SP_TP, None),
            P(SP_TP, None),
            P(SP, None, "tp"),
            P(SP, None, "tp"),
            P(SP, "tp", None),
        ),
        out_specs=P(SP_TP, None),
        check_vma=False,
    )
```

time: 759 us -> 226 us (0.30)
  matrix products: 252 us -> 19.8 us
  other arithmetic: 183 us -> 5.19 us
  waiting for transfers between devices: 204 us -> 114 us
  Pallas kernels: 0 us -> 43.5 us
  local copies, waits for them, and re-layouts: 54.5 us -> 23.2 us
  blocking collectives: 35.8 us -> 8.06 us
  between operations: 14.9 us -> 0.19 us
    dot_general x57 -> x2, matrix products: 231 us -> 0.48 us  [the longest x1 0.35 us: local(): jnp.dot(back_map, returned.reshape(capacity * experts, width), preferred_...]
    another operation x9 -> x0, other arithmetic: 167 us -> none  [the longest x5 161 us: block_terms(): lax.linalg.triangular_solve(system, sources, left_side=True, lower=True,...]
    all_gather x6 -> x0, waiting for transfers between devices: 107 us -> none  [entering_2(): pieces = jax.tree.map(lambda part: lax.all_gather(part, axis), total)]
    pallas_call x0 -> x2, Pallas kernels: none -> 43.5 us  [the longest x1 34.1 us: mixer_finish(): pl.pallas_call(functools.partial(mixer_finish_kernel, experts), in_specs=...]
    all_to_all x2 -> x0, blocking collectives: 27.8 us -> none  [the longest x1 23.4 us: local(): lax.all_to_all(expert_out, SP_TP, split_axis=0, concat_axis=2, tiled=True)]
    all_to_all x0 -> x1, waiting for transfers between devices: none -> 17.4 us  [local(): lax.all_to_all(expert_out, SP_TP, split_axis=0, concat_axis=2, tiled=True)]
    dynamic_update_slice x24 -> x0, local copies, waits for them, and re-layouts: 15.1 us -> none  [local(): lax.scan(across_blocks, (identity, nothing), (block_map, block_state))]
    unnamed x120 -> x19, local copies, waits for them, and re-layouts: 15.4 us -> 11.8 us
  transfers between devices with their start and end apart: 8 -> 3, of which waited for: 8 -> 3; matrix products, arithmetic and copies ran while one was open for 11% -> 2% of each run, Pallas kernels for 0% -> 0%
where the time goes in v1:
time: 226 us; the launch traced here: 225 us
  waiting for transfers between devices  114 us (50%)
  Pallas kernels  43.5 us (19%)
  local copies, waits for them, and re-layouts  23.2 us (10%)
  matrix products  19.8 us (9%)
  starting transfers between devices  11.8 us (5%)
  blocking collectives  8.06 us (4%)
  other arithmetic  5.19 us (2%)
    all_to_all x1, waiting for transfers between devices, local(): lax.all_to_all(copies.reshape(peers * capacity, width), SP_TP, split_axis...  52.5 us
    ppermute x1, waiting for transfers between devices, from_partner(): lax.ppermute(array, axis, [(i, i ^ 1 << bit) for i in range(lax.axis_size...  43.7 us
    pallas_call x1, Pallas kernels, mixer_finish(): pl.pallas_call(functools.partial(mixer_finish_kernel, experts), in_specs=...  34.1 us
    all_to_all x1, waiting for transfers between devices, local(): lax.all_to_all(expert_out, SP_TP, split_axis=0, concat_axis=2, tiled=True)  17.4 us
    unnamed x19, local copies, waits for them, and re-layouts  11.8 us
    pallas_call x1, Pallas kernels, mixer_blocks(): pl.pallas_call(functools.partial(mixer_kernel, per_step), grid=(pairs //...  9.34 us
    all_to_all x1, blocking collectives, sent_and_summed(): lax.all_to_all(split_up(array, dim, length), axis, 0, 0, tiled=True)  8.06 us
    all_to_all x1, starting transfers between devices, local(): lax.all_to_all(copies.reshape(peers * capacity, width), SP_TP, split_axis...  7.99 us
  transfers between devices with their start and end apart: 3, of which 3 were waited for; matrix products, arithmetic and copies ran while one was open for 2% of the time, Pallas kernels for 0%

profile of v1, /device:TPU:1, one launch (start us, length us, event | category | flops | bytes accessed | tf_op | source)
XLA Modules:
  0.0 225.3 jit_solution(5261435464336933845)
XLA Ops:
  0.0 0.7 reshape.70.gain_ref
  0.7 0.7 reshape.71.ffn_gain_ref
  1.4 0.8 copy.77.routes_ref
  2.1 9.3 %mixer_blocks.1 = (f32[8,128,128]{2,1,0:T(8,128)}, f32[128,1024]{1,0:T(8,128)}, f32[128,1024]{1,0:T(8,128)}) custom-call(bf16[128,1024]{1,0:T(8,128)(2,1)} %q_ref.1, bf16[128,1024]{1,0:T(8,128)(2,1)} %k_ref.1, bf16[128,1024]{1,0:T(8,128)(2,1)} %v_ref.1, bf16[128,1024]{1,0:T(8,128)(2,1)} %r_ref.1, bf16[128,1024]{1,0:T(8,128)(2,1)} %l_ref.1, f32[128,1024]{1,0:T(8,128)} %g_ref.1), custom_call_target="tpu_custom_call" | custom-call | tf_op jit(solution)/shard_map/mixer_blocks/pallas_call | solution.py:183
  11.5 0.0 copy-start
  11.5 1.0 copy-done
  12.5 0.0 copy-start.1
  12.5 1.0 copy-done.1
  13.6 0.0 copy-start.2
  13.6 1.0 copy-done.2
  14.6 0.0 copy-start.3
  14.6 0.9 copy-done.3
  15.6 34.1 %mixer_finish.1 = (f32[64,2048]{1,0:T(8,128)S(1)}, bf16[256,2048]{1,0:T(8,128)(2,1)S(1)}) custom-call(f32[8,128,128]{2,1,0:T(8,128)S(1)} %copy-done, f32[128,1024]{1,0:T(8,128)S(1)} %copy-done.1, f32[128,1024]{1,0:T(8,128)S(1)} %copy-done.2, bf16[1,1024]{1,0:T(2,128)(2,1)S(1)} %reshape.70.gain_ref, bf16[64,2048]{1,0:T(8,128)(2,1)S(1)} %copy-done.3, ...), custom_call_target="tpu_custom_call" | custom-call | tf_op jit(solution)/shard_map/mixer_finish/pallas_call | solution.py:436
  49.7 2.5 %broadcast_in_dim.10 = bf16[32,4,8,2048]{3,2,1,0:T(8,128)(2,1)} broadcast(bf16[32,8,2048]{2,1,0:T(8,128)(2,1)S(1)} %bitcast.40), dimensions={0,2,3} | broadcast | bytes 5242880 | tf_op jit(solution)/shard_map/broadcast_in_dim | solution.py:527
  52.2 8.0 %all-to-all-start = ((bf16[128,8,2048]{2,1,0:T(8,128)(2,1)}), bf16[128,8,2048]{2,1,0:T(8,128)(2,1)}, u32[]{:S(2)}, u32[]{:S(2)}) async-start(bf16[128,8,2048]{2,1,0:T(8,128)(2,1)} %bitcast.41), calls=%async_computation | async-start | bytes 8388608 | tf_op jit(solution)/shard_map/all_to_all | solution.py:530
  60.2 52.5 %all-to-all-done = bf16[128,8,2048]{2,1,0:T(8,128)(2,1)} async-done(((bf16[128,8,2048]{2,1,0:T(8,128)(2,1)}), bf16[128,8,2048]{2,1,0:T(8,128)(2,1)}, u32[]{:S(2)}, u32[]{:S(2)}) %all-to-all-start) | async-done | bytes 4194336 | tf_op jit(solution)/shard_map/all_to_all | solution.py:530
  112.8 0.0 copy-start.6
  112.8 7.5 %fusion = f32[1024,896]{1,0:T(8,128)S(1)} fusion(bf16[128,8,2048]{2,1,0:T(8,128)(2,1)} %all-to-all-done, bf16[1,2048,896]{2,1,0:T(8,128)(2,1)} %param.28), kind=kOutput, calls=%fused_computation.1 | convolution fusion | flops 3758096384 | bytes 11534336 | tf_op jit(solution)/shard_map/dot_general | solution.py:534
  120.3 0.0 copy-done.6
  120.3 0.0 copy-start.7
  120.3 7.1 %multiply_convert_fusion = bf16[1024,896]{1,0:T(8,128)(2,1)S(1)} fusion(f32[1024,896]{1,0:T(8,128)S(1)} %fusion, bf16[1,2048,896]{2,1,0:T(8,128)(2,1)S(1)} %copy-done.6, bf16[128,8,2048]{2,1,0:T(8,128)(2,1)} %all-to-all-done), kind=kOutput, calls=%fused_computation.10 | convolution fusion | flops 3763601408 | bytes 13369344 | tf_op jit(solution)/shard_map/dot_general | solution.py:533
  127.4 0.0 copy-done.7
  127.4 4.7 %convert_bitcast_fusion = bf16[128,8,2048]{2,1,0:T(8,128)(2,1)S(1)} fusion(bf16[1024,896]{1,0:T(8,128)(2,1)S(1)} %multiply_convert_fusion, bf16[1,896,2048]{2,1,0:T(8,128)(2,1)S(1)} %copy-done.7), kind=kOutput, calls=%fused_computation.6 | convolution fusion | flops 3760193536 | bytes 9699328 | tf_op jit(solution)/shard_map/dot_general | solution.py:536
  132.1 1.8 constant_dynamic-slice_fusion.1
  133.9 4.1 %copy.87 = bf16[128,8,1024]{0,2,1:T(8,128)(2,1)} copy(bf16[128,8,1024]{2,1,0:T(8,128)(2,1)} %get-tuple-element.16) | data formatting | bytes 4194304
  138.0 0.0 collective-permute-start
  138.0 2.8 %copy.86 = bf16[128,8,1024]{0,2,1:T(8,128)(2,1)} copy(bf16[128,8,1024]{2,1,0:T(8,128)(2,1)S(1)} %get-tuple-element.15) | data formatting | bytes 4194304
  140.9 43.7 %collective-permute-done = bf16[128,8,1024]{0,2,1:T(8,128)(2,1)} collective-permute-done((bf16[128,8,1024]{0,2,1:T(8,128)(2,1)}, bf16[128,8,1024]{0,2,1:T(8,128)(2,1)}, u32[]{:S(2)}, u32[]{:S(2)}) %collective-permute-start) | collective-permute-done | bytes 2097184 | tf_op jit(solution)/shard_map/ppermute | solution.py:477
  184.6 2.8 %add_convert_fusion = bf16[128,8,1024]{0,2,1:T(8,128)(2,1)S(1)} fusion(bf16[128,8,1024]{0,2,1:T(8,128)(2,1)} %collective-permute-done, bf16[128,8,1024]{0,2,1:T(8,128)(2,1)} %copy.86), kind=kLoop, calls=%fused_computation.5 | loop fusion | flops 4194304 | bytes 6291456 | tf_op jit(solution)/shard_map/convert_element_type | solution.py:546
  187.4 3.0 %copy.82 = bf16[2,128,8,512]{3,2,1,0:T(8,128)(2,1)} copy(bf16[2,128,8,512]{1,3,0,2:T(8,128)(2,1)S(1)} %bitcast.42) | data formatting | bytes 4194304 | tf_op jit(solution)/shard_map/transpose | solution.py:482
  190.3 8.1 %all_to_all.32 = bf16[2,128,8,512]{3,2,1,0:T(8,128)(2,1)S(1)} all-to-all(bf16[2,128,8,512]{3,2,1,0:T(8,128)(2,1)} %copy.82), channel_id=1, replica_groups=mesh['grp'=8,'mem'=8,'tp'=2] {'tp'}, dimensions={0} | all-to-all | bytes 4194304 | tf_op jit(solution)/shard_map/all_to_all | solution.py:487
  198.4 0.0 copy-start.4
  198.4 1.6 reduce_sum.21
  200.0 3.8 %all-to-all-start.2 = ((bf16[128,8,512]{2,1,0:T(8,128)(2,1)}), bf16[128,8,512]{2,1,0:T(8,128)(2,1)S(1)}, u32[]{:S(2)}, u32[]{:S(2)}) async-start(bf16[128,8,512]{2,1,0:T(8,128)(2,1)} %reduce_sum.21), calls=%async_computation.2 | async-start | bytes 2097152 | tf_op jit(solution)/shard_map/all_to_all | solution.py:547
  203.8 0.0 copy-done.4
  203.9 0.1 copy.78
  204.0 0.1 reshape.75
  204.1 0.1 convolution_convert_fusion
  204.2 1.3 gather_fusion
  205.6 0.0 copy-start.5
  205.6 0.1 reshape.78
  205.7 0.1 copy.79
  205.8 17.4 %all-to-all-done.2 = bf16[128,8,512]{2,1,0:T(8,128)(2,1)S(1)} async-done(((bf16[128,8,512]{2,1,0:T(8,128)(2,1)}), bf16[128,8,512]{2,1,0:T(8,128)(2,1)S(1)}, u32[]{:S(2)}, u32[]{:S(2)}) %all-to-all-start.2) | async-done | bytes 1048608 | tf_op jit(solution)/shard_map/all_to_all | solution.py:547
  223.2 0.3 copy.84
  223.5 0.7 reshape.86
  224.2 0.0 copy-done.5
  224.2 0.4 fusion.11
  224.6 0.8 add_convert_fusion.1
  (3 shorter events, 0.0 us)
Async XLA Ops:
  11.5 1.0 copy-start
  12.5 1.0 copy-start.1
  13.6 1.0 copy-start.2
  14.6 0.9 copy-start.3
  52.2 60.6 %all-to-all-start = ((bf16[128,8,2048]{2,1,0:T(8,128)(2,1)}), bf16[128,8,2048]{2,1,0:T(8,128)(2,1)}, u32[]{:S(2)}, u32[]{:S(2)}) async-start(bf16[128,8,2048]{2,1,0:T(8,128)(2,1)} %bitcast.41), calls=%async_computation | async-start | bytes 8388608 | tf_op jit(solution)/shard_map/all_to_all | solution.py:530
  112.8 7.5 %copy-start.6 = (bf16[1,2048,896]{2,1,0:T(8,128)(2,1)S(1)}, bf16[1,2048,896]{2,1,0:T(8,128)(2,1)}, u32[]{:S(2)}) copy-start(bf16[1,2048,896]{2,1,0:T(8,128)(2,1)} %param.27) | copy-start | bytes 11010052
  120.3 7.1 %copy-start.7 = (bf16[1,896,2048]{2,1,0:T(8,128)(2,1)S(1)}, bf16[1,896,2048]{2,1,0:T(8,128)(2,1)}, u32[]{:S(2)}) copy-start(bf16[1,896,2048]{2,1,0:T(8,128)(2,1)} %param.29) | copy-start | bytes 11010052
  138.0 46.5 %collective-permute-start = (bf16[128,8,1024]{0,2,1:T(8,128)(2,1)}, bf16[128,8,1024]{0,2,1:T(8,128)(2,1)}, u32[]{:S(2)}, u32[]{:S(2)}) collective-permute-start(bf16[128,8,1024]{0,2,1:T(8,128)(2,1)} %copy.87), channel_id=1, source_target_pairs={{0,2},{2,0},{4,6},{6,4},{8,10},{10,8},{12,14},{14,12},{16,18},{18,... | collective-permute-start | bytes 6291464 | tf_op jit(solution)/shard_map/ppermute | solution.py:477
  198.4 5.4 %copy-start.4 = (s32[64,2]{0,1:T(2,128)S(1)}, s32[64,2]{0,1:T(2,128)}, u32[]{:S(2)}) copy-start(s32[64,2]{0,1:T(2,128)} %param.25) | copy-start | bytes 1540
  200.0 23.2 %all-to-all-start.2 = ((bf16[128,8,512]{2,1,0:T(8,128)(2,1)}), bf16[128,8,512]{2,1,0:T(8,128)(2,1)S(1)}, u32[]{:S(2)}, u32[]{:S(2)}) async-start(bf16[128,8,512]{2,1,0:T(8,128)(2,1)} %reduce_sum.21), calls=%async_computation.2 | async-start | bytes 2097152 | tf_op jit(solution)/shard_map/all_to_all | solution.py:547
  205.6 18.6 %copy-start.5 = (f32[64,2]{0,1:T(2,128)S(1)}, f32[64,2]{0,1:T(2,128)}, u32[]{:S(2)}) copy-start(f32[64,2]{0,1:T(2,128)} %param.26) | copy-start | bytes 1540

commit v2 on v1

--- a/solution.py
+++ b/solution.py
@@ -1,4 +1,5 @@
 import functools
+import math
 from typing import NamedTuple
 
 import jax
@@ -468,24 +469,251 @@
     )(z, local_read, carry_read, gain, stream, weight, ffn_gain, routes)
 
 
+PLANES = 4
+
+
+def plane_offset(step):
+    return step + step // 2 * (1 - 2 * (step % 2))
+
+
+def experts_kernel(
+    dispatched_ref,
+    attended_ref,
+    routes_ref,
+    share_ref,
+    gate_ref,
+    up_ref,
+    down_ref,
+    out_ref,
+    rows,
+    gate,
+    up,
+    down,
+    hidden,
+    part,
+    part_got,
+    back_out,
+    back,
+    fetch_sems,
+    own_sems,
+    row_sent,
+    row_got,
+    pass_sent,
+    pass_got,
+    part_sent,
+    part_got_sem,
+    back_sent,
+    back_got,
+):
+    group, member, core = (lax.axis_index(a) for a in ("grp", "mem", "tp"))
+    members = lax.axis_size("mem")
+    chips, experts = back.shape[1], dispatched_ref.shape[0]
+    capacity, width = rows.shape[3:]
+    floor = chips // PLANES
+    side = math.isqrt(floor)
+    half_width = width // 2
+    chip = group * members + member
+    plane, spot = chip // floor, chip % floor
+
+    def at(target, which):
+        return (target // members, lax.rem(target, members), which)
+
+    def spot_of(offset):
+        return lax.rem(spot // side + offset // side, side) * side + lax.rem(
+            lax.rem(spot, side) + lax.rem(offset, side), side
+        )
+
+    barrier = pltpu.get_barrier_semaphore()
+    devices = 2 * chips
+
+    def greet(offset, carry):
+        peer = lax.rem(2 * chip + core + offset, devices)
+        pl.semaphore_signal(
+            barrier, inc=1, device_id=at(peer // 2, lax.rem(peer, 2)), device_id_type=MESH
+        )
+        return carry
+
+    lax.fori_loop(1, devices, greet, 0)
+    fetches = []
+    for n, (source, target) in enumerate(((gate_ref, gate), (up_ref, up), (down_ref, down))):
+        fetches.append(pltpu.make_async_copy(source.at[0], target, fetch_sems.at[n]))
+        fetches[-1].start()
+    own_rows = pltpu.make_async_copy(
+        dispatched_ref.at[chip // 2], rows.at[core, plane, spot], own_sems.at[0]
+    )
+    own_rows.start()
+    pl.semaphore_wait(barrier, devices - 1)
+
+    for step in range(PLANES):
+        target_plane = lax.rem(plane + plane_offset(step), PLANES)
+
+        def send_rows(offset, carry):
+            target = target_plane * floor + spot_of(offset)
+            remote(
+                dispatched_ref.at[target // 2],
+                rows.at[core, plane, spot],
+                row_sent.at[step],
+                row_got.at[step],
+                at(target, core),
+            ).start()
+            return carry
+
+        lax.fori_loop(1 if step == 0 else 0, floor, send_rows, 0)
+
+    own_rows.wait()
+    for copy in fetches:
+        copy.wait()
+
+    def row_copies(step, source_plane, count):
+        span = rows.at[core, source_plane, pl.ds(0, count)]
+        return remote(span, span, row_sent.at[step], row_got.at[step], at(chip, 1 - core))
+
+    def passing(step, source_plane, side_core):
+        span = rows.at[side_core, source_plane]
+        return remote(span, span, pass_sent.at[step], pass_got.at[step], at(chip, 1 - core))
+
+    def part_copy(step):
+        return remote(
+            part.at[step, 1 - core],
+            part_got.at[step],
+            part_sent.at[step],
+            part_got_sem.at[step],
+            at(chip, 1 - core),
+        )
+
+    def back_copy(step, source_plane, which, offset):
+        target = source_plane * floor + spot_of(offset)
+        return remote(
+            back_out.at[step, which, lax.rem(target, floor)],
+            back.at[core, chip],
+            back_sent.at[step],
+            back_got.at[core],
+            at(target, which),
+        )
+
+    def plane_of(step):
+        return lax.rem(plane + PLANES - plane_offset(step), PLANES)
+
+    def compute(step, source_plane):
+        held = rows[:, source_plane].reshape(2 * floor * capacity, width)
+        inner = gate.shape[1]
+        for start in range(0, inner, 256):
+            lanes = slice(start, min(start + 256, inner))
+            gate_act = mxu(held, gate[:, lanes])
+            up_act = mxu(held, up[:, lanes])
+            hidden[:, lanes] = (gate_act * jax.nn.sigmoid(gate_act) * up_act).astype(BF16)
+        for side_at in range(2):
+            for start in range(0, half_width, 512):
+                lanes = slice(start, min(start + 512, half_width))
+                columns = slice(side_at * half_width + lanes.start, side_at * half_width + lanes.stop)
+                part[step, side_at, :, lanes] = mxu(hidden[...], down[:, columns]).astype(BF16)
+
+    def finish(step):
+        source_plane = plane_of(step)
+        part_copy(step).wait_recv()
+        total = part[step, core].astype(F32) + part_got[step].astype(F32)
+        back_out[step] = total.astype(BF16).reshape(2, floor, capacity, half_width)
+
+        def send_back(offset, carry):
+            back_copy(step, source_plane, 1 - core, offset).start()
+            return carry
+
+        def send_same(offset, carry):
+            back_copy(step, source_plane, core, offset).start()
+            return carry
+
+        lax.fori_loop(0, floor, send_back, 0)
+        if isinstance(step, int) and step == 0:
+            lax.fori_loop(1, floor, send_same, 0)
+            own = pltpu.make_async_copy(
+                back_out.at[0, core, spot], back.at[core, chip], own_sems.at[1]
+            )
+            own.start()
+            own.wait()
+        else:
+            lax.fori_loop(0, floor, send_same, 0)
+
+    for step in range(PLANES):
+        source_plane = plane_of(step)
+        row_copies(step, source_plane, floor - 1 if step == 0 else floor).wait_recv()
+        passing(step, source_plane, core).start()
+        passing(step, source_plane, 1 - core).wait_recv()
+        compute(step, source_plane)
+        part_copy(step).start()
+        if step > 0:
+            finish(step - 1)
+    finish(PLANES - 1)
+
+    kept, named = slot_map(routes_ref, experts, capacity)
+    shares = kept * jnp.where(named[0], share_ref[:, 0:1], share_ref[:, 1:2])
+    shares = packed(split(shares))
+    for turn in range(2):
+        which = 1 - core if turn == 0 else core
+        span = back.at[which, pl.ds(0, chips - turn)]
+        remote(span, span, back_sent.at[0], back_got.at[which], at(chip, 1 - core)).wait_recv()
+    for which in range(2):
+        lanes = slice(which * half_width, (which + 1) * half_width)
+        pair = back[which].reshape(experts, 2, capacity, half_width).astype(F32)
+        whole = (pair[:, 0] + pair[:, 1]).astype(BF16).reshape(experts * capacity, half_width)
+        mixture = mxu(shares, jnp.concatenate((whole, whole), axis=0))
+        out_ref[:, lanes] = (attended_ref[:, lanes] + mixture).astype(BF16)
+
+    for step in range(PLANES):
+        source_plane = plane_of(step)
+        row_copies(step, source_plane, floor - 1 if step == 0 else floor).wait_send()
+        passing(step, source_plane, core).wait_send()
+        part_copy(step).wait_send()
+        if step == 0:
+            sent = back_out.at[step, 0]
+            remote(sent, sent, back_sent.at[step], back_got.at[0], at(chip, 1 - core)).wait_send()
+            if floor > 1:
+                sent = back_out.at[step, 0, pl.ds(0, floor - 1)]
+                remote(sent, sent, back_sent.at[step], back_got.at[0], at(chip, 1 - core)).wait_send()
+        else:
+            sent = back_out.at[step]
+            remote(sent, sent, back_sent.at[step], back_got.at[0], at(chip, 1 - core)).wait_send()
+
+
+def routed_experts(dispatched, attended, routes, shares, gate, up, down):
+    experts, capacity, width = dispatched.shape
+    half = attended.shape[0]
+    chips = 2 * experts
+    inner = gate.shape[2]
+    floor = chips // PLANES
+    rows_step = 2 * floor * capacity
+    vmem = pl.BlockSpec(memory_space=pltpu.VMEM)
+    hbm = pl.BlockSpec(memory_space=pl.ANY)
+    dma = pltpu.SemaphoreType.DMA
+    return pl.pallas_call(
+        experts_kernel,
+        in_specs=[vmem] * 4 + [hbm] * 3,
+        out_specs=vmem,
+        out_shape=jax.ShapeDtypeStruct((half, width), BF16),
+        scratch_shapes=[
+            pltpu.VMEM((2, PLANES, floor, capacity, width), BF16),
+            pltpu.VMEM((width, inner), BF16),
+            pltpu.VMEM((width, inner), BF16),
+            pltpu.VMEM((inner, width), BF16),
+            pltpu.VMEM((rows_step, inner), BF16),
+            pltpu.VMEM((PLANES, 2, rows_step, width // 2), BF16),
+            pltpu.VMEM((PLANES, rows_step, width // 2), BF16),
+            pltpu.VMEM((PLANES, 2, floor, capacity, width // 2), BF16),
+            pltpu.VMEM((2, chips, capacity, width // 2), BF16),
+            dma((3,)),
+            dma((2,)),
+        ]
+        + [dma((PLANES,))] * 7
+        + [dma((2,))],
+        compiler_params=pltpu.CompilerParams(
+            collective_id=1, has_side_effects=True, vmem_limit_bytes=58 * 1024 * 1024
+        ),
+        name="routed_experts",
+    )(dispatched, attended, routes, shares, gate, up, down)
+
+
 TOPK = 2
 SP_TP = ("grp", "mem", "tp")
 SP = ("grp", "mem")
-
-
-def from_partner(array, axis, bit):
-    return lax.ppermute(array, axis, [(i, i ^ 1 << bit) for i in range(lax.axis_size(axis))])
-
-
-def split_up(array, dim, length):
-    before, after = (array.shape[:dim], array.shape[dim + 1 :])
-    return jnp.moveaxis(array.reshape(*before, length, -1, *after), dim, 0)
-
-
-def sent_and_summed(array, axis, dim):
-    length = lax.axis_size(axis)
-    pieces = lax.all_to_all(split_up(array, dim, length), axis, 0, 0, tiled=True)
-    return jnp.sum(pieces.astype(jnp.float32), axis=0)
 
 
 def local(
@@ -507,7 +735,6 @@
 ):
     half_rows, width = stream_in.shape
     experts = lax.axis_size(SP) // 2
-    peers = lax.axis_size(SP_TP)
     capacity = 2 * TOPK * half_rows // experts
     z, local_read, carry_read = mixer_blocks(
         query_rows, key_rows, value_rows, removal_key, learn_pre, log_rate, per_step=4
@@ -524,42 +751,15 @@
         experts,
         capacity,
     )
-    copies = jnp.broadcast_to(
-        dispatched.reshape(experts, 1, capacity, width), (experts, 4, capacity, width)
-    )
-    routed = lax.all_to_all(
-        copies.reshape(peers * capacity, width), SP_TP, split_axis=0, concat_axis=0, tiled=True
-    )
-    gate_act = jnp.dot(routed, expert_gate[0], preferred_element_type=jnp.float32)
-    up_act = jnp.dot(routed, expert_up[0], preferred_element_type=jnp.float32)
-    hidden = (jax.nn.silu(gate_act) * up_act).astype(jnp.bfloat16)
-    partial_out = jnp.dot(hidden, expert_down[0], preferred_element_type=jnp.float32).astype(
-        jnp.bfloat16
-    )
-    partial_out = partial_out.reshape(peers, capacity, width)
-    pair_bit = lax.axis_index(SP) % 2
-    half_width = width // 2
-    kept_half = lax.dynamic_slice_in_dim(partial_out, pair_bit * half_width, half_width, 2)
-    sent_half = lax.dynamic_slice_in_dim(partial_out, (1 - pair_bit) * half_width, half_width, 2)
-    partner_half = from_partner(sent_half, SP, 0)
-    pair_sum = kept_half.astype(jnp.float32) + partner_half.astype(jnp.float32)
-    expert_out = sent_and_summed(pair_sum.astype(jnp.bfloat16), "tp", 2).astype(jnp.bfloat16)
-    returned = lax.all_to_all(expert_out, SP_TP, split_axis=0, concat_axis=2, tiled=True)
-    returned = returned.reshape(capacity, experts, width)
-    lane = jnp.arange(experts, dtype=jnp.int32)
-    one_hot = (routes[:, :, None] == lane).any(axis=1)
-    earlier = jnp.arange(half_rows)[:, None] > jnp.arange(half_rows)[None, :]
-    place = jnp.dot(earlier.astype(jnp.float32), one_hot.astype(jnp.float32))
-    slot = jnp.take_along_axis(place.astype(jnp.int32), routes, axis=1).reshape(-1)
-    back_index = slot * experts + routes.reshape(-1)
-    back_map = (
-        back_index[:, None] == jnp.arange(capacity * experts, dtype=jnp.int32)[None, :]
-    ).astype(jnp.bfloat16)
-    picked = jnp.dot(
-        back_map, returned.reshape(capacity * experts, width), preferred_element_type=jnp.float32
-    ).reshape(half_rows, TOPK, width)
-    mixture = jnp.sum(picked * route_weight[:, :, None], axis=1)
-    return (attended + mixture).astype(jnp.bfloat16)
+    return routed_experts(
+        dispatched.reshape(experts, capacity, width),
+        attended,
+        routes,
+        route_weight,
+        expert_gate,
+        expert_up,
+        expert_down,
+    )
 
 
 def solution(mesh):

time: 226 us -> 130 us (0.58)
  waiting for transfers between devices: 114 us -> 0 us
  Pallas kernels: 43.5 us -> 119 us
  matrix products: 19.8 us -> 0 us
  local copies, waits for them, and re-layouts: 23.2 us -> 10.4 us
  starting transfers between devices: 11.8 us -> 0 us
  blocking collectives: 8.06 us -> 0 us
  other arithmetic: 5.19 us -> 0 us
    pallas_call x0 -> x1, Pallas kernels: none -> 75.6 us  [routed_experts(): pl.pallas_call(experts_kernel, in_specs=[vmem] * 4 + [hbm] * 3, out_specs...]
    all_to_all x2 -> x0, waiting for transfers between devices: 69.9 us -> none  [the longest x1 52.5 us: local(): lax.all_to_all(copies.reshape(peers * capacity, width), SP_TP, split_axis...]
    ppermute x1 -> x0, waiting for transfers between devices: 43.7 us -> none  [from_partner(): lax.ppermute(array, axis, [(i, i ^ 1 << bit) for i in range(lax.axis_size...]
    dot_general x5 -> x0, matrix products: 19.8 us -> none  [the longest x1 7.49 us: local(): up_act = jnp.dot(routed, expert_up[0], preferred_element_type=jnp.float32)]
    all_to_all x2 -> x0, starting transfers between devices: 11.8 us -> none  [the longest x1 7.99 us: local(): lax.all_to_all(copies.reshape(peers * capacity, width), SP_TP, split_axis...]
    all_to_all x1 -> x0, blocking collectives: 8.06 us -> none  [sent_and_summed(): lax.all_to_all(split_up(array, dim, length), axis, 0, 0, tiled=True)]
    convert_element_type x2 -> x0, other arithmetic: 3.52 us -> none  [the longest x1 2.77 us: local(): pair_sum.astype(jnp.bfloat16)]
    transpose x1 -> x0, local copies, waits for them, and re-layouts: 2.97 us -> none  [split_up(): return jnp.moveaxis(array.reshape(*before, length, -1, *after), dim, 0)]
  transfers between devices with their start and end apart: 3 -> 0, of which waited for: 3 -> 0; matrix products, arithmetic and copies ran while one was open for 2% -> 0% of each run, Pallas kernels for 0% -> 0%
where the time goes in v2:
time: 130 us; the launch traced here: 129 us
  Pallas kernels  119 us (92%)
  local copies, waits for them, and re-layouts  10.4 us (8%)
    pallas_call x1, Pallas kernels, routed_experts(): pl.pallas_call(experts_kernel, in_specs=[vmem] * 4 + [hbm] * 3, out_specs...  75.6 us
    pallas_call x1, Pallas kernels, mixer_finish(): pl.pallas_call(functools.partial(mixer_finish_kernel, experts), in_specs=...  34.1 us
    pallas_call x1, Pallas kernels, mixer_blocks(): pl.pallas_call(functools.partial(mixer_kernel, per_step), grid=(pairs //...  9.35 us
    unnamed x19, local copies, waits for them, and re-layouts  8.99 us

profile of v2, /device:TPU:1, one launch (start us, length us, event | category | flops | bytes accessed | tf_op | source)
XLA Modules:
  0.0 129.5 jit_solution(13269470308242269240)
XLA Ops:
  0.0 9.3 %mixer_blocks.1 = (f32[8,128,128]{2,1,0:T(8,128)}, f32[128,1024]{1,0:T(8,128)}, f32[128,1024]{1,0:T(8,128)}) custom-call(bf16[128,1024]{1,0:T(8,128)(2,1)} %q_ref.1, bf16[128,1024]{1,0:T(8,128)(2,1)} %k_ref.1, bf16[128,1024]{1,0:T(8,128)(2,1)} %v_ref.1, bf16[128,1024]{1,0:T(8,128)(2,1)} %r_ref.1, bf16[128,1024]{1,0:T(8,128)(2,1)} %l_ref.1, f32[128,1024]{1,0:T(8,128)} %g_ref.1), custom_call_target="tpu_custom_call" | custom-call | tf_op jit(solution)/shard_map/mixer_blocks/pallas_call | solution.py:184
  9.3 0.8 copy.16.routes_ref
  10.1 0.0 copy-start.5
  10.1 0.7 reshape.10.ffn_gain_ref
  10.8 0.7 reshape.9.gain_ref
  11.5 0.0 copy-start.2
  11.5 1.0 copy-done.2
  12.6 0.0 copy-start.3
  12.6 1.0 copy-done.3
  13.6 0.0 copy-start.4
  13.6 1.0 copy-done.4
  14.6 0.0 copy-start.6
  14.6 0.9 copy-done.6
  15.6 0.0 copy-start.7
  15.6 34.1 %mixer_finish.1 = (f32[64,2048]{1,0:T(8,128)S(1)}, bf16[256,2048]{1,0:T(8,128)(2,1)S(1)}) custom-call(f32[8,128,128]{2,1,0:T(8,128)S(1)} %copy-done.2, f32[128,1024]{1,0:T(8,128)S(1)} %copy-done.3, f32[128,1024]{1,0:T(8,128)S(1)} %copy-done.4, bf16[1,1024]{1,0:T(2,128)(2,1)S(1)} %reshape.9.gain_ref, bf16[64,2048]{1,0:T(8,128)(2,1)S(1)} %copy-done.6, ...), custom_call_target="tpu_custom_call" | custom-call | tf_op jit(solution)/shard_map/mixer_finish/pallas_call | solution.py:437
  49.7 0.0 copy-done.5
  49.7 0.0 copy-start
  49.7 1.0 copy-done
  50.7 0.0 copy-start.1
  50.7 0.8 copy-done.1
  51.5 0.0 copy-done.7
  51.5 0.7 copy.18.share_ref
  52.2 75.6 %routed_experts.1 = bf16[64,2048]{1,0:T(8,128)(2,1)} custom-call(bf16[32,8,2048]{2,1,0:T(8,128)(2,1)} %bitcast.1, f32[64,2048]{1,0:T(8,128)} %copy-done.1, s32[64,2]{1,0:T(8,128)} %copy-done.5, f32[64,2]{1,0:T(8,128)} %copy.18.share_ref, bf16[1,2048,896]{2,1,0:T(8,128)(2,1)} %gate_ref.1, bf16[1,2048,896]{2,1,0:T(8,128)(2,1)} %up_ref.1, ...), custom_call_target="tpu_custom_call" | custom-call | tf_op jit(solution)/shard_map/routed_experts/pallas_call | solution.py:687
  127.8 1.7 %copy.20 = bf16[64,2048]{1,0:T(8,128)(2,1)} copy(bf16[64,2048]{1,0:T(8,128)(2,1)} %routed_experts.1) | data formatting | bytes 524288
Async XLA Ops:
  10.1 39.6 %copy-start.5 = (s32[64,2]{1,0:T(8,128)}, s32[64,2]{1,0:T(8,128)S(1)}, u32[]{:S(2)}) copy-start(s32[64,2]{1,0:T(8,128)S(1)} %copy.16.routes_ref) | copy-start | bytes 1540
  11.5 1.0 copy-start.2
  12.6 1.0 copy-start.3
  13.6 1.0 copy-start.4
  14.6 0.9 copy-start.6
  15.6 35.9 %copy-start.7 = (f32[64,2]{0,1:T(2,128)S(1)}, f32[64,2]{0,1:T(2,128)}, u32[]{:S(2)}) copy-start(f32[64,2]{0,1:T(2,128)} %param.26) | copy-start | bytes 1540
  49.7 1.0 copy-start
  50.7 0.8 copy-start.1

commit v3 on v1

--- a/solution.py
+++ b/solution.py
@@ -1,4 +1,3 @@
-import functools
 from typing import NamedTuple
 
 import jax
@@ -176,24 +175,6 @@
         )
 
 
-def mixer_blocks(queries, keys, values, removal, learn, rates, per_step=2):
-    tokens, width = queries.shape
-    pairs = width // LANES
-    rows = pl.BlockSpec((tokens, per_step * LANES), lambda i: (0, i))
-    return pl.pallas_call(
-        functools.partial(mixer_kernel, per_step),
-        grid=(pairs // per_step,),
-        in_specs=[rows] * 6,
-        out_specs=[pl.BlockSpec((per_step, 2 * HEAD, LANES), lambda i: (i, 0, 0)), rows, rows],
-        out_shape=[
-            jax.ShapeDtypeStruct((pairs, 2 * HEAD, LANES), F32),
-            jax.ShapeDtypeStruct((tokens, width), F32),
-            jax.ShapeDtypeStruct((tokens, width), F32),
-        ],
-        name="mixer_blocks",
-    )(queries, keys, values, removal, learn, rates)
-
-
 MESH = pl.DeviceIdType.MESH
 GROUP_EPS = 0.00064
 NORM_EPS = 1e-06
@@ -322,13 +303,15 @@
     same_head = ((iota((LANES, LANES), 0) < HEAD) == (iota((LANES, LANES), 1) < HEAD)).astype(BF16)
     same_head = jnp.concatenate((same_head, same_head), axis=0)
     pairs = entered.shape[0]
+    per_step = pairs // local_ref.shape[0]
     lanes = [slice(pair * LANES, (pair + 1) * LANES) for pair in range(pairs)]
     mixed = []
     for pair in range(pairs):
         high, low = split(block_diagonal(entered[pair]))
         rhs = jnp.concatenate((packed((high, high)), packed((low, low))), axis=0)
-        read = folded(mxu(packed(split(carry_ref[:, lanes[pair]])), rhs, ((1,), (1,))))
-        mixed.append(local_ref[:, lanes[pair]] + read)
+        step, held = pair // per_step, lanes[pair % per_step]
+        read = folded(mxu(packed(split(carry_ref[step, :, held])), rhs, ((1,), (1,))))
+        mixed.append(local_ref[step, :, held] + read)
     centred = [x - mxu(packed(split(x)), same_head) * (1.0 / HEAD) for x in mixed]
     variance = [mxu(packed(split(x * x)), same_head) * (1.0 / HEAD) for x in centred]
     for pair in range(pairs):
@@ -337,155 +320,305 @@
 
 
 def slot_map(routes_ref, experts, capacity):
-    half = routes_ref.shape[0]
-    shape = (half, experts * capacity)
-    lane = iota(shape, 1)
-    expert, slot = lane // capacity, lane % capacity
-    named = [routes_ref[:, k : k + 1] == expert for k in range(2)]
+    half = routes_ref.shape[1]
+    shape = (experts * capacity, half)
+    place = iota(shape, 0)
+    expert, slot = place // capacity, place % capacity
+    named = [routes_ref[k : k + 1, :] == expert for k in range(2)]
     chosen = (named[0] | named[1]).astype(F32)
-    earlier = (iota((half, half), 0) > iota((half, half), 1)).astype(BF16)
-    place = mxu(earlier, chosen.astype(BF16))
-    kept = jnp.where(place == slot.astype(F32), chosen, 0.0)
-    return kept, named
-
-
-def mixer_finish_kernel(
-    experts,
-    z_ref,
-    local_ref,
-    carry_ref,
-    gain_ref,
+    earlier = (iota((half, half), 0) < iota((half, half), 1)).astype(BF16)
+    count = mxu(chosen.astype(BF16), earlier)
+    return jnp.where(count == slot.astype(F32), chosen, 0.0), named
+
+
+SP_TP = ("grp", "mem", "tp")
+SP = ("grp", "mem")
+STEPS = 2
+GROUPS = 4
+
+
+def far_first(side):
+    offsets = [(z, y, x) for z in range(side) for y in range(side) for x in range(side)]
+    return sorted(offsets, key=lambda o: -sum(min(d, side - d) for d in o))
+
+
+def layer_kernel(
+    q_ref,
+    k_ref,
+    v_ref,
+    r_ref,
+    l_ref,
+    g_ref,
     stream_ref,
     weight_ref,
+    gate_ref,
+    up_ref,
+    down_ref,
+    gain_ref,
     ffn_gain_ref,
     routes_ref,
-    attended_ref,
-    dispatched_ref,
+    share_ref,
+    out_ref,
+    q,
+    k,
+    v,
+    r,
+    l,
+    g,
+    stream,
+    weight,
+    gate,
+    up,
+    down,
+    z,
+    local_read,
+    carry_read,
     by_member,
     by_group,
     total_ref,
     found,
     entered,
     normed,
-    weight,
     partial,
     other,
-    weight_sem,
+    attended,
+    dispatched,
+    rows,
+    hidden,
+    part,
+    part_got,
+    back_out,
+    back,
+    in_sems,
+    fetch_sems,
+    sent_1,
+    got_1,
+    sent_2,
+    got_2,
+    sent_3,
+    got_3,
     sent_4,
     got_4,
-    *sems,
+    row_sent,
+    row_got,
+    pass_sent,
+    pass_got,
+    part_sent,
+    part_arrived,
+    back_sent,
+    back_got,
 ):
     group, member, core = (lax.axis_index(a) for a in ("grp", "mem", "tp"))
-    members, groups = by_member.shape[0], by_group.shape[0]
+    members = lax.axis_size("mem")
+    chips, experts = back.shape[1], dispatched.shape[0]
+    capacity, width = rows.shape[2:]
+    half_width = width // 2
+    chip = group * members + member
+    sibling = (group, member, 1 - core)
+
+    def at(target, which):
+        return (target // members, lax.rem(target, members), which)
+
     barrier = pltpu.get_barrier_semaphore()
-    peers = [(group, lax.rem(member + o, members), core) for o in range(1, members)]
-    peers += [(lax.rem(group + o, groups), member, core) for o in range(1, groups)]
-    peers += [(group, member, 1 - core)]
-    for peer in peers:
-        pl.semaphore_signal(barrier, inc=1, device_id=peer, device_id_type=MESH)
+    devices = 2 * chips
+
+    def greet(offset, carry):
+        peer = lax.rem(2 * chip + core + offset, devices)
+        pl.semaphore_signal(
+            barrier, inc=1, device_id=at(peer // 2, lax.rem(peer, 2)), device_id_type=MESH
+        )
+        return carry
+
+    held = q.shape[2]
+    loads = []
+    for step in range(STEPS):
+        lanes = pl.ds(step * held, held)
+        for n, (source, target) in enumerate(
+            ((q_ref, q), (k_ref, k), (v_ref, v), (r_ref, r), (l_ref, l), (g_ref, g))
+        ):
+            loads.append(
+                pltpu.make_async_copy(source.at[:, lanes], target.at[step], in_sems.at[step, n])
+            )
+            loads[-1].start()
     depth = weight.shape[0]
-    fetch = pltpu.make_async_copy(weight_ref.at[pl.ds(core * depth, depth)], weight, weight_sem)
-    fetch.start()
-    pl.semaphore_wait(barrier, len(peers))
-
-    copies = entering_states(z_ref, by_member, by_group, total_ref, found, entered, sems)
-    normed_heads(local_ref, carry_ref, entered, gain_ref, normed)
-    fetch.wait()
-    half = stream_ref.shape[0]
+    fetches = []
+    for n, (source, target) in enumerate(
+        (
+            (stream_ref, stream),
+            (weight_ref.at[pl.ds(core * depth, depth)], weight),
+            (gate_ref.at[0], gate),
+            (up_ref.at[0], up),
+            (down_ref.at[0], down),
+        )
+    ):
+        fetches.append(pltpu.make_async_copy(source, target, fetch_sems.at[n]))
+    lax.fori_loop(1, devices, greet, 0)
+    for copy in loads[: len(loads) // STEPS]:
+        copy.wait()
+    for copy in fetches:
+        copy.start()
+
+    pairs = z.shape[0] // STEPS
+
+    def mix(step):
+        mixer_kernel(
+            pairs,
+            *(ref.at[step] for ref in (q, k, v, r, l, g)),
+            z.at[pl.ds(step * pairs, pairs)],
+            local_read.at[step],
+            carry_read.at[step],
+        )
+
+    mix(0)
+    for copy in loads[len(loads) // STEPS :]:
+        copy.wait()
+    mix(1)
+    pl.semaphore_wait(barrier, devices - 1)
+
+    sems = (sent_1, got_1, sent_2, got_2, sent_3, got_3)
+    copies = entering_states(z, by_member, by_group, total_ref, found, entered, sems)
+    normed_heads(local_read, carry_read, entered, gain_ref, normed)
+    fetches[0].wait()
+    fetches[1].wait()
+    half = stream.shape[0]
     chunks = partial.shape[0]
     mine, theirs = pl.ds(core * half, half), pl.ds((1 - core) * half, half)
+    shared = []
     for n in range(chunks):
         partial[n] = jnp.dot(
             normed[...], weight[:, n * COLUMNS : (n + 1) * COLUMNS], preferred_element_type=F32
         )
-        copy = remote(
-            partial.at[n, theirs],
-            other.at[n],
-            sent_4.at[n],
-            got_4.at[n],
-            (group, member, 1 - core),
-        )
-        copy.start()
-        copies.append(copy)
-    kept, _ = slot_map(routes_ref, experts, dispatched_ref.shape[0] // experts)
-    kept = kept.astype(BF16)
+        shared.append(
+            remote(partial.at[n, theirs], other.at[n], sent_4.at[n], got_4.at[n], sibling)
+        )
+        shared[-1].start()
+    kept, named = slot_map(routes_ref, experts, capacity)
+    picks = kept.astype(BF16)
+    shares = kept * jnp.where(named[0], share_ref[0:1, :], share_ref[1:2, :])
+    shares = jnp.concatenate(split(shares), axis=0)
     squares = jnp.zeros((half, 1), F32)
     for n in range(chunks):
         lanes = slice(n * COLUMNS, (n + 1) * COLUMNS)
-        copies[n - chunks].wait_recv()
-        attended = stream_ref[:, lanes].astype(F32) + (partial[n, mine] + other[n])
-        attended_ref[:, lanes] = attended
-        squares = squares + jnp.sum(attended * attended, axis=1, keepdims=True)
-    width = chunks * COLUMNS
+        shared[n].wait_recv()
+        block = stream[:, lanes].astype(F32) + (partial[n, mine] + other[n])
+        attended[:, lanes] = block
+        squares = squares + jnp.sum(block * block, axis=1, keepdims=True)
     scaling = lax.rsqrt(squares * (1.0 / width) + NORM_EPS)
     for n in range(chunks):
         lanes = slice(n * COLUMNS, (n + 1) * COLUMNS)
-        ffn_in = attended_ref[:, lanes] * scaling * ffn_gain_ref[:, lanes].astype(F32)
-        dispatched_ref[:, lanes] = mxu(kept, ffn_in.astype(BF16), ((0,), (0,))).astype(BF16)
-    for copy in copies:
+        ffn_in = attended[:, lanes] * scaling * ffn_gain_ref[:, lanes].astype(F32)
+        sent_rows = mxu(picks, ffn_in.astype(BF16)).astype(BF16)
+        dispatched[:, :, lanes] = sent_rows.reshape(experts, capacity, COLUMNS)
+
+    side = round(chips ** (1 / 3))
+    order = far_first(side)
+    here = (chip // (side * side), chip // side % side, chip % side)
+
+    def shifted(offset, sign):
+        place = [lax.rem(h + side + sign * o, side) for h, o in zip(here, offset)]
+        return (place[0] * side + place[1]) * side + place[2]
+
+    span = chips // GROUPS
+    rows[core, chips - 1] = dispatched[chip // 2]
+    for n, offset in enumerate(order[:-1]):
+        target = shifted(offset, 1)
+        remote(
+            dispatched.at[target // 2],
+            rows.at[core, n],
+            row_sent.at[n // span],
+            row_got.at[n // span],
+            at(target, core),
+        ).start()
+    for copy in fetches[2:]:
+        copy.wait()
+
+    def row_copies(step):
+        count = span - 1 if step == GROUPS - 1 else span
+        held = rows.at[core, pl.ds(step * span, count)]
+        return remote(held, held, row_sent.at[step], row_got.at[step], sibling)
+
+    def passing(step, which):
+        held = rows.at[which, pl.ds(step * span, span)]
+        return remote(held, held, pass_sent.at[step], pass_got.at[step], sibling)
+
+    def part_copy(step):
+        return remote(
+            part.at[step, 1 - core],
+            part_got.at[step],
+            part_sent.at[step],
+            part_arrived.at[step],
+            sibling,
+        )
+
+    def compute(step):
+        taken = rows[:, step * span : (step + 1) * span].reshape(2 * span * capacity, width)
+        inner = gate.shape[1]
+        for start in range(0, inner, 256):
+            lanes = slice(start, min(start + 256, inner))
+            gate_act = mxu(taken, gate[:, lanes])
+            up_act = mxu(taken, up[:, lanes])
+            hidden[:, lanes] = (gate_act * jax.nn.sigmoid(gate_act) * up_act).astype(BF16)
+        for which in range(2):
+            for start in range(0, half_width, COLUMNS):
+                columns = slice(which * half_width + start, which * half_width + start + COLUMNS)
+                part[step, which, :, start : start + COLUMNS] = mxu(
+                    hidden[...], down[:, columns]
+                ).astype(BF16)
+
+    def finish(step):
+        part_copy(step).wait_recv()
+        total = part[step, core].astype(F32) + part_got[step].astype(F32)
+        back_out[step] = total.astype(BF16).reshape(2, span, capacity, half_width)
+        for n in range(span):
+            offset = order[step * span + n]
+            target = shifted(offset, -1)
+            for turn in range(2):
+                which = 1 - core if turn == 0 else core
+                if turn == 1 and not any(offset):
+                    back[core, chip] = back_out[step, core, n]
+                    continue
+                remote(
+                    back_out.at[step, which, n],
+                    back.at[core, chip],
+                    back_sent.at[step],
+                    back_got.at[core],
+                    at(target, which),
+                ).start()
+
+    for step in range(GROUPS):
+        row_copies(step).wait_recv()
+        passing(step, core).start()
+        passing(step, 1 - core).wait_recv()
+        compute(step)
+        part_copy(step).start()
+        if step > 0:
+            finish(step - 1)
+    finish(GROUPS - 1)
+
+    def all_back(ref, sem_sent, sem_got):
+        return remote(ref, ref, sem_sent, sem_got, sibling)
+
+    for turn in range(2):
+        which = 1 - core if turn == 0 else core
+        all_back(back.at[which, pl.ds(0, chips - turn)], back_sent.at[0], back_got.at[which]).wait_recv()
+    for which in range(2):
+        lanes = slice(which * half_width, (which + 1) * half_width)
+        both = back[which].reshape(experts, 2, capacity, half_width).astype(F32)
+        whole = (both[:, 0] + both[:, 1]).astype(BF16).reshape(experts * capacity, half_width)
+        mixture = mxu(shares, jnp.concatenate((whole, whole), axis=0), ((0,), (0,)))
+        out_ref[:, lanes] = (attended[:, lanes] + mixture).astype(BF16)
+
+    for copy in copies + shared:
         copy.wait_send()
-
-
-def mixer_finish(z, local_read, carry_read, gain, stream, weight, ffn_gain, routes, experts, capacity):
-    half, width = stream.shape
-    tokens = local_read.shape[0]
-    members, groups = lax.axis_size("mem"), lax.axis_size("grp")
-    chunks = width // COLUMNS
-    vmem = pl.BlockSpec(memory_space=pltpu.VMEM)
-    dma = pltpu.SemaphoreType.DMA
-    return pl.pallas_call(
-        functools.partial(mixer_finish_kernel, experts),
-        in_specs=[vmem] * 5 + [pl.BlockSpec(memory_space=pl.ANY)] + [vmem] * 2,
-        out_specs=[vmem, vmem],
-        out_shape=[
-            jax.ShapeDtypeStruct((half, width), F32),
-            jax.ShapeDtypeStruct((experts * capacity, width), BF16),
-        ],
-        scratch_shapes=[
-            pltpu.VMEM((members, 2 * HEAD, LANES), F32),
-            pltpu.VMEM((groups, 2 * HEAD, LANES), F32),
-            pltpu.VMEM((2 * HEAD, LANES), F32),
-            pltpu.VMEM((members, HEAD, LANES), F32),
-            pltpu.VMEM((members, HEAD, LANES), F32),
-            pltpu.VMEM((tokens, width // 2), BF16),
-            pltpu.VMEM((width // 2, width), BF16),
-            pltpu.VMEM((chunks, tokens, COLUMNS), F32),
-            pltpu.VMEM((chunks, half, COLUMNS), F32),
-            dma,
-            dma((chunks,)),
-            dma((chunks,)),
-            dma((members,)),
-            dma((members,)),
-            dma((groups,)),
-            dma((groups,)),
-            dma((members,)),
-            dma((members,)),
-        ],
-        compiler_params=pltpu.CompilerParams(
-            collective_id=0, has_side_effects=True, vmem_limit_bytes=48 * 1024 * 1024
-        ),
-        name="mixer_finish",
-    )(z, local_read, carry_read, gain, stream, weight, ffn_gain, routes)
-
-
-TOPK = 2
-SP_TP = ("grp", "mem", "tp")
-SP = ("grp", "mem")
-
-
-def from_partner(array, axis, bit):
-    return lax.ppermute(array, axis, [(i, i ^ 1 << bit) for i in range(lax.axis_size(axis))])
-
-
-def split_up(array, dim, length):
-    before, after = (array.shape[:dim], array.shape[dim + 1 :])
-    return jnp.moveaxis(array.reshape(*before, length, -1, *after), dim, 0)
-
-
-def sent_and_summed(array, axis, dim):
-    length = lax.axis_size(axis)
-    pieces = lax.all_to_all(split_up(array, dim, length), axis, 0, 0, tiled=True)
-    return jnp.sum(pieces.astype(jnp.float32), axis=0)
+    for step in range(GROUPS):
+        row_copies(step).wait_send()
+        passing(step, core).wait_send()
+        part_copy(step).wait_send()
+        last = 1 if step == GROUPS - 1 else 0
+        all_back(back_out.at[step, 0], back_sent.at[step], back_got.at[0]).wait_send()
+        all_back(
+            back_out.at[step, 1, pl.ds(0, span - last)], back_sent.at[step], back_got.at[0]
+        ).wait_send()
 
 
 def local(
@@ -505,61 +638,87 @@
     expert_up,
     expert_down,
 ):
-    half_rows, width = stream_in.shape
-    experts = lax.axis_size(SP) // 2
-    peers = lax.axis_size(SP_TP)
-    capacity = 2 * TOPK * half_rows // experts
-    z, local_read, carry_read = mixer_blocks(
-        query_rows, key_rows, value_rows, removal_key, learn_pre, log_rate, per_step=4
-    )
-    attended, dispatched = mixer_finish(
-        z,
-        local_read,
-        carry_read,
-        norm_gain.reshape(1, -1),
+    half, width = stream_in.shape
+    tokens, own_width = query_rows.shape
+    chips = lax.axis_size(("grp", "mem"))
+    members, groups = lax.axis_size("mem"), lax.axis_size("grp")
+    experts = chips // 2
+    capacity = 2 * routes.shape[1] * half // experts
+    inner = expert_gate.shape[2]
+    span = chips // GROUPS
+    held = own_width // STEPS
+    pairs = own_width // LANES
+    chunks = width // COLUMNS
+    taken = 2 * span * capacity
+    vmem = pl.BlockSpec(memory_space=pltpu.VMEM)
+    hbm = pl.BlockSpec(memory_space=pl.ANY)
+    dma = pltpu.SemaphoreType.DMA
+    return pl.pallas_call(
+        layer_kernel,
+        in_specs=[hbm] * 11 + [vmem] * 4,
+        out_specs=vmem,
+        out_shape=jax.ShapeDtypeStruct((half, width), BF16),
+        scratch_shapes=[pltpu.VMEM((STEPS, tokens, held), BF16)] * 5
+        + [
+            pltpu.VMEM((STEPS, tokens, held), F32),
+            pltpu.VMEM((half, width), BF16),
+            pltpu.VMEM((width // 2, width), BF16),
+            pltpu.VMEM((width, inner), BF16),
+            pltpu.VMEM((width, inner), BF16),
+            pltpu.VMEM((inner, width), BF16),
+            pltpu.VMEM((pairs, 2 * HEAD, LANES), F32),
+            pltpu.VMEM((STEPS, tokens, held), F32),
+            pltpu.VMEM((STEPS, tokens, held), F32),
+            pltpu.VMEM((members, 2 * HEAD, LANES), F32),
+            pltpu.VMEM((groups, 2 * HEAD, LANES), F32),
+            pltpu.VMEM((2 * HEAD, LANES), F32),
+            pltpu.VMEM((members, HEAD, LANES), F32),
+            pltpu.VMEM((members, HEAD, LANES), F32),
+            pltpu.VMEM((tokens, own_width), BF16),
+            pltpu.VMEM((chunks, tokens, COLUMNS), F32),
+            pltpu.VMEM((chunks, half, COLUMNS), F32),
+            pltpu.VMEM((half, width), F32),
+            pltpu.VMEM((experts, capacity, width), BF16),
+            pltpu.VMEM((2, chips, capacity, width), BF16),
+            pltpu.VMEM((taken, inner), BF16),
+            pltpu.VMEM((GROUPS, 2, taken, width // 2), BF16),
+            pltpu.VMEM((GROUPS, taken, width // 2), BF16),
+            pltpu.VMEM((GROUPS, 2, span, capacity, width // 2), BF16),
+            pltpu.VMEM((2, chips, capacity, width // 2), BF16),
+            dma((STEPS, 6)),
+            dma((5,)),
+            dma((members,)),
+            dma((members,)),
+            dma((groups,)),
+            dma((groups,)),
+            dma((members,)),
+            dma((members,)),
+            dma((chunks,)),
+            dma((chunks,)),
+        ]
+        + [dma((GROUPS,))] * 7
+        + [dma((2,))],
+        compiler_params=pltpu.CompilerParams(
+            collective_id=0, has_side_effects=True, vmem_limit_bytes=63 * 1024 * 1024
+        ),
+        name="layer",
+    )(
+        query_rows,
+        key_rows,
+        value_rows,
+        removal_key,
+        learn_pre,
+        log_rate,
         stream_in,
         out_weight,
+        expert_gate,
+        expert_up,
+        expert_down,
+        norm_gain.reshape(1, -1),
         ffn_gain.reshape(1, -1),
-        routes,
-        experts,
-        capacity,
+        routes.T,
+        route_weight.T,
     )
-    copies = jnp.broadcast_to(
-        dispatched.reshape(experts, 1, capacity, width), (experts, 4, capacity, width)
-    )
-    routed = lax.all_to_all(
-        copies.reshape(peers * capacity, width), SP_TP, split_axis=0, concat_axis=0, tiled=True
-    )
-    gate_act = jnp.dot(routed, expert_gate[0], preferred_element_type=jnp.float32)
-    up_act = jnp.dot(routed, expert_up[0], preferred_element_type=jnp.float32)
-    hidden = (jax.nn.silu(gate_act) * up_act).astype(jnp.bfloat16)
-    partial_out = jnp.dot(hidden, expert_down[0], preferred_element_type=jnp.float32).astype(
-        jnp.bfloat16
-    )
-    partial_out = partial_out.reshape(peers, capacity, width)
-    pair_bit = lax.axis_index(SP) % 2
-    half_width = width // 2
-    kept_half = lax.dynamic_slice_in_dim(partial_out, pair_bit * half_width, half_width, 2)
-    sent_half = lax.dynamic_slice_in_dim(partial_out, (1 - pair_bit) * half_width, half_width, 2)
-    partner_half = from_partner(sent_half, SP, 0)
-    pair_sum = kept_half.astype(jnp.float32) + partner_half.astype(jnp.float32)
-    expert_out = sent_and_summed(pair_sum.astype(jnp.bfloat16), "tp", 2).astype(jnp.bfloat16)
-    returned = lax.all_to_all(expert_out, SP_TP, split_axis=0, concat_axis=2, tiled=True)
-    returned = returned.reshape(capacity, experts, width)
-    lane = jnp.arange(experts, dtype=jnp.int32)
-    one_hot = (routes[:, :, None] == lane).any(axis=1)
-    earlier = jnp.arange(half_rows)[:, None] > jnp.arange(half_rows)[None, :]
-    place = jnp.dot(earlier.astype(jnp.float32), one_hot.astype(jnp.float32))
-    slot = jnp.take_along_axis(place.astype(jnp.int32), routes, axis=1).reshape(-1)
-    back_index = slot * experts + routes.reshape(-1)
-    back_map = (
-        back_index[:, None] == jnp.arange(capacity * experts, dtype=jnp.int32)[None, :]
-    ).astype(jnp.bfloat16)
-    picked = jnp.dot(
-        back_map, returned.reshape(capacity * experts, width), preferred_element_type=jnp.float32
-    ).reshape(half_rows, TOPK, width)
-    mixture = jnp.sum(picked * route_weight[:, :, None], axis=1)
-    return (attended + mixture).astype(jnp.bfloat16)
 
 
 def solution(mesh):

time: 226 us -> 108 us (0.48)
  waiting for transfers between devices: 114 us -> 0 us
  Pallas kernels: 43.5 us -> 102 us
  matrix products: 19.8 us -> 0 us
  local copies, waits for them, and re-layouts: 23.2 us -> 4.23 us
  starting transfers between devices: 11.8 us -> 0 us
  blocking collectives: 8.06 us -> 0 us
  other arithmetic: 5.19 us -> 0 us
    all_to_all x2 -> x0, waiting for transfers between devices: 69.9 us -> none  [the longest x1 52.5 us: local(): lax.all_to_all(copies.reshape(peers * capacity, width), SP_TP, split_axis...]
    pallas_call x2 -> x1, Pallas kernels: 43.5 us -> 102 us  [local(): pl.pallas_call(layer_kernel, in_specs=[hbm] * 11 + [vmem] * 4, out_specs=...]
    ppermute x1 -> x0, waiting for transfers between devices: 43.7 us -> none  [from_partner(): lax.ppermute(array, axis, [(i, i ^ 1 << bit) for i in range(lax.axis_size...]
    dot_general x5 -> x0, matrix products: 19.8 us -> none  [the longest x1 7.49 us: local(): up_act = jnp.dot(routed, expert_up[0], preferred_element_type=jnp.float32)]
    all_to_all x2 -> x0, starting transfers between devices: 11.8 us -> none  [the longest x1 7.99 us: local(): lax.all_to_all(copies.reshape(peers * capacity, width), SP_TP, split_axis...]
    unnamed x19 -> x1, local copies, waits for them, and re-layouts: 11.8 us -> 1.67 us
    all_to_all x1 -> x0, blocking collectives: 8.06 us -> none  [sent_and_summed(): lax.all_to_all(split_up(array, dim, length), axis, 0, 0, tiled=True)]
    convert_element_type x2 -> x0, other arithmetic: 3.52 us -> none  [the longest x1 2.77 us: local(): pair_sum.astype(jnp.bfloat16)]
  transfers between devices with their start and end apart: 3 -> 0, of which waited for: 3 -> 0; matrix products, arithmetic and copies ran while one was open for 2% -> 0% of each run, Pallas kernels for 0% -> 0%
where the time goes in v3:
time: 108 us; the launch traced here: 106 us
  Pallas kernels  102 us (94%)
  local copies, waits for them, and re-layouts  4.23 us (4%)
    pallas_call x1, Pallas kernels, local(): pl.pallas_call(layer_kernel, in_specs=[hbm] * 11 + [vmem] * 4, out_specs=...  102 us

profile of v3, /device:TPU:1, one launch (start us, length us, event | category | flops | bytes accessed | tf_op | source)
XLA Modules:
  0.0 105.8 jit_solution(11324365057802391801)
XLA Ops:
  0.0 1.3 %reshape.6.gain_ref = bf16[1,1024]{1,0:T(2,128)(2,1)} reshape(bf16[1024]{0:T(1024)(128)(2,1)} %param.22) | data formatting | bytes 4096 | tf_op jit(solution)/shard_map/reshape | solution.py:717
  1.3 1.3 %reshape.7.ffn_gain_ref = bf16[1,2048]{1,0:T(2,128)(2,1)} reshape(bf16[2048]{0:T(1024)(128)(2,1)} %param.24) | data formatting | bytes 8192 | tf_op jit(solution)/shard_map/reshape | solution.py:718
  2.6 101.5 %layer.1 = bf16[64,2048]{1,0:T(8,128)(2,1)} custom-call(bf16[128,1024]{1,0:T(8,128)(2,1)} %q_ref.1, bf16[128,1024]{1,0:T(8,128)(2,1)} %k_ref.1, bf16[128,1024]{1,0:T(8,128)(2,1)} %v_ref.1, bf16[128,1024]{1,0:T(8,128)(2,1)} %r_ref.1, bf16[128,1024]{1,0:T(8,128)(2,1)} %l_ref.1, f32[128,1024]{1,0:T(8,128)} %g_ref.1, bf16[64,2048]{1,0:T(8,128)(2,1)} %stream_ref.1, ...), custom_call_target="tpu_custom_call" | custom-call | tf_op jit(solution)/shard_map/layer/pallas_call | solution.py:656
  104.1 1.7 %copy.17 = bf16[64,2048]{1,0:T(8,128)(2,1)} copy(bf16[64,2048]{1,0:T(8,128)(2,1)} %layer.1) | data formatting | bytes 524288

commit v4 on v3

--- a/solution.py
+++ b/solution.py
@@ -169,10 +169,11 @@
         written = mxu(ready[pair].values, ready[pair].key_tail, ((0,), (0,)))
         z_ref[pair, :HEAD] = jnp.where(
             half, written[:HEAD] - outer[one][:HEAD], written[HEAD:] - outer[two][HEAD:]
-        )
-        z_ref[pair, HEAD:] = jnp.where(diagonal, ready[pair].decay_all, 0.0) - jnp.where(
+        ).astype(BF16)
+        changed = jnp.where(diagonal, ready[pair].decay_all - 1.0, 0.0) - jnp.where(
             half, outer[one][HEAD:], outer[two][:HEAD]
         )
+        z_ref[pair, HEAD:] = changed.astype(BF16)
 
 
 MESH = pl.DeviceIdType.MESH
@@ -187,13 +188,9 @@
     return jnp.concatenate((jnp.where(first, rows, zero), jnp.where(first, zero, rows)), axis=0)
 
 
-def mapped(earlier, later):
-    return product(split(earlier), split(block_diagonal(later[HEAD:])))
-
-
 def compose(earlier, later):
-    joined = mapped(earlier, later)
-    return jnp.concatenate((joined[:HEAD] + later[:HEAD], joined[HEAD:]), axis=0)
+    turned = product(split(earlier), split(block_diagonal(later[HEAD:])))
+    return turned + earlier + later
 
 
 def prefixes(blocks):
@@ -224,33 +221,44 @@
     )
 
 
-def entering_states(z_ref, by_member, by_group, total_ref, found, entered, sems):
+def member_copies(z, by_member, sent, got, part, parts):
+    group, member, core = (lax.axis_index(a) for a in ("grp", "mem", "tp"))
+    count = by_member.shape[0] // parts
+    copies = []
+    for offset in range(count):
+        peer = part * count + lax.rem(member + offset, count)
+        copy = remote(
+            z.at[peer], by_member.at[member], sent.at[peer], got.at[member], (group, peer, core)
+        )
+        copies.append((peer != member, copy))
+    return copies
+
+
+def start_all(copies):
+    for away, copy in copies:
+        pl.when(away)(copy.start)
+
+
+def sent_all(copies):
+    for away, copy in copies:
+        pl.when(away)(copy.wait_send)
+
+
+def entering_states(z, by_member, by_group, total_ref, found, entered, sems):
     group, member, core = (lax.axis_index(a) for a in ("grp", "mem", "tp"))
     members, groups = by_member.shape[0], by_group.shape[0]
-    sent_1, got_1, sent_2, got_2, sent_3, got_3 = sems
-
-    first = []
-    for offset in range(1, members):
-        peer = lax.rem(member + offset, members)
-        copy = remote(
-            z_ref.at[peer],
-            by_member.at[member],
-            sent_1.at[offset],
-            got_1.at[member],
-            (group, peer, core),
-        )
-        copy.start()
-        first.append(copy)
-    by_member[member] = z_ref[member]
+    got_1, sent_2, got_2, sent_3, got_3 = sems
+
+    by_member[member] = z[member]
     for offset in range(1, members):
         peer = lax.rem(member + offset, members)
         remote(
-            z_ref.at[peer], by_member.at[peer], sent_1.at[offset], got_1.at[peer], (group, peer, core)
+            z.at[peer], by_member.at[peer], sent_3.at[offset], got_1.at[peer], (group, peer, core)
         ).wait_recv()
-    inclusive = prefixes([by_member[j] for j in range(members)])
-    total_ref[...] = inclusive[-1]
-
-    second = []
+    inclusive = prefixes([by_member[j].astype(F32) for j in range(members)])
+    total_ref[...] = inclusive[-1].astype(BF16)
+
+    copies = []
     for offset in range(1, groups):
         peer = lax.rem(group + offset, groups)
         copy = remote(
@@ -261,7 +269,7 @@
             (peer, member, core),
         )
         copy.start()
-        second.append(copy)
+        copies.append(copy)
     maps = [spread(split(block_diagonal(inclusive[j][HEAD:]))) for j in range(members - 1)]
     by_group[group] = total_ref[...]
     for offset in range(1, groups):
@@ -269,16 +277,14 @@
         remote(
             total_ref, by_group.at[peer], sent_2.at[offset], got_2.at[peer], (peer, member, core)
         ).wait_recv()
-    shape = total_ref.shape
-    neutral = ((iota(shape, 1) % HEAD) + HEAD == iota(shape, 0)).astype(F32)
-    before = [jnp.where(j < group, by_group[j], neutral) for j in range(groups - 1)]
+    before = [jnp.where(j < group, by_group[j].astype(F32), 0.0) for j in range(groups - 1)]
     start = joined_all(before)[:HEAD]
     parts = packed(split(start))
-    found[0] = start
+    found[0] = start.astype(BF16)
     for j in range(1, members):
-        found[j] = folded(mxu(parts, maps[j - 1])) + inclusive[j - 1][:HEAD]
-
-    third = []
+        turned = folded(mxu(parts, maps[j - 1]))
+        found[j] = (turned + start + inclusive[j - 1][:HEAD]).astype(BF16)
+
     for offset in range(1, members):
         peer = lax.rem(member + offset, members)
         copy = remote(
@@ -289,14 +295,14 @@
             (group, peer, core),
         )
         copy.start()
-        third.append(copy)
+        copies.append(copy)
     entered[member] = found[member]
     for offset in range(1, members):
         peer = lax.rem(member + offset, members)
         remote(
             found.at[peer], entered.at[peer], sent_3.at[offset], got_3.at[peer], (group, peer, core)
         ).wait_recv()
-    return first + second + third
+    return copies
 
 
 def normed_heads(local_ref, carry_ref, entered, gain_ref, normed):
@@ -307,10 +313,10 @@
     lanes = [slice(pair * LANES, (pair + 1) * LANES) for pair in range(pairs)]
     mixed = []
     for pair in range(pairs):
-        high, low = split(block_diagonal(entered[pair]))
-        rhs = jnp.concatenate((packed((high, high)), packed((low, low))), axis=0)
+        state = block_diagonal(entered[pair])
         step, held = pair // per_step, lanes[pair % per_step]
-        read = folded(mxu(packed(split(carry_ref[step, :, held])), rhs, ((1,), (1,))))
+        carry = packed(split(carry_ref[step, :, held]))
+        read = mxu(carry, packed((state, state)), ((1,), (1,)))
         mixed.append(local_ref[step, :, held] + read)
     centred = [x - mxu(packed(split(x)), same_head) * (1.0 / HEAD) for x in mixed]
     variance = [mxu(packed(split(x * x)), same_head) * (1.0 / HEAD) for x in centred]
@@ -334,7 +340,8 @@
 SP_TP = ("grp", "mem", "tp")
 SP = ("grp", "mem")
 STEPS = 2
-GROUPS = 4
+BOUNDS = (0, 16, 32, 48, 64)
+GROUPS = len(BOUNDS) - 1
 
 
 def far_first(side):
@@ -470,12 +477,16 @@
         )
 
     mix(0)
+    pl.semaphore_wait(barrier, devices - 1)
+    early = member_copies(z, by_member, sent_1, got_1, 0, STEPS)
+    start_all(early)
     for copy in loads[len(loads) // STEPS :]:
         copy.wait()
     mix(1)
-    pl.semaphore_wait(barrier, devices - 1)
-
-    sems = (sent_1, got_1, sent_2, got_2, sent_3, got_3)
+    late = member_copies(z, by_member, sent_1, got_1, 1, STEPS)
+    start_all(late)
+
+    sems = (got_1, sent_2, got_2, sent_3, got_3)
     copies = entering_states(z, by_member, by_group, total_ref, found, entered, sems)
     normed_heads(local_read, carry_read, entered, gain_ref, normed)
     fetches[0].wait()
@@ -518,67 +529,75 @@
         place = [lax.rem(h + side + sign * o, side) for h, o in zip(here, offset)]
         return (place[0] * side + place[1]) * side + place[2]
 
-    span = chips // GROUPS
     rows[core, chips - 1] = dispatched[chip // 2]
     for n, offset in enumerate(order[:-1]):
         target = shifted(offset, 1)
         remote(
             dispatched.at[target // 2],
             rows.at[core, n],
-            row_sent.at[n // span],
-            row_got.at[n // span],
+            row_sent.at[sum(n >= b for b in BOUNDS[1:])],
+            row_got.at[sum(n >= b for b in BOUNDS[1:])],
             at(target, core),
         ).start()
     for copy in fetches[2:]:
         copy.wait()
 
     def row_copies(step):
-        count = span - 1 if step == GROUPS - 1 else span
-        held = rows.at[core, pl.ds(step * span, count)]
+        start, stop = BOUNDS[step : step + 2]
+        held = rows.at[core, pl.ds(start, min(stop, chips - 1) - start)]
         return remote(held, held, row_sent.at[step], row_got.at[step], sibling)
 
     def passing(step, which):
-        held = rows.at[which, pl.ds(step * span, span)]
+        start, stop = BOUNDS[step : step + 2]
+        held = rows.at[which, pl.ds(start, stop - start)]
         return remote(held, held, pass_sent.at[step], pass_got.at[step], sibling)
 
+    def taken_rows(step):
+        start, stop = BOUNDS[step : step + 2]
+        return slice(2 * start * capacity, 2 * stop * capacity)
+
     def part_copy(step):
+        taken = taken_rows(step)
+        taken = pl.ds(taken.start, taken.stop - taken.start)
         return remote(
-            part.at[step, 1 - core],
-            part_got.at[step],
+            part.at[1 - core, taken],
+            part_got.at[taken],
             part_sent.at[step],
             part_arrived.at[step],
             sibling,
         )
 
     def compute(step):
-        taken = rows[:, step * span : (step + 1) * span].reshape(2 * span * capacity, width)
+        start, stop = BOUNDS[step : step + 2]
+        count = 2 * (stop - start) * capacity
+        taken = rows[:, start:stop].reshape(count, width)
         inner = gate.shape[1]
-        for start in range(0, inner, 256):
-            lanes = slice(start, min(start + 256, inner))
+        for begin in range(0, inner, 256):
+            lanes = slice(begin, min(begin + 256, inner))
             gate_act = mxu(taken, gate[:, lanes])
             up_act = mxu(taken, up[:, lanes])
-            hidden[:, lanes] = (gate_act * jax.nn.sigmoid(gate_act) * up_act).astype(BF16)
+            hidden[:count, lanes] = (gate_act * jax.nn.sigmoid(gate_act) * up_act).astype(BF16)
         for which in range(2):
-            for start in range(0, half_width, COLUMNS):
-                columns = slice(which * half_width + start, which * half_width + start + COLUMNS)
-                part[step, which, :, start : start + COLUMNS] = mxu(
-                    hidden[...], down[:, columns]
+            for begin in range(0, half_width, COLUMNS):
+                columns = slice(which * half_width + begin, which * half_width + begin + COLUMNS)
+                part[which, taken_rows(step), begin : begin + COLUMNS] = mxu(
+                    hidden[:count], down[:, columns]
                 ).astype(BF16)
 
     def finish(step):
         part_copy(step).wait_recv()
-        total = part[step, core].astype(F32) + part_got[step].astype(F32)
-        back_out[step] = total.astype(BF16).reshape(2, span, capacity, half_width)
-        for n in range(span):
-            offset = order[step * span + n]
-            target = shifted(offset, -1)
+        start, stop = BOUNDS[step : step + 2]
+        total = part[core, taken_rows(step)].astype(F32) + part_got[taken_rows(step)].astype(F32)
+        back_out[:, start:stop] = total.astype(BF16).reshape(2, stop - start, capacity, half_width)
+        for n in range(start, stop):
+            target = shifted(order[n], -1)
             for turn in range(2):
                 which = 1 - core if turn == 0 else core
-                if turn == 1 and not any(offset):
-                    back[core, chip] = back_out[step, core, n]
+                if turn == 1 and not any(order[n]):
+                    back[core, chip] = back_out[core, n]
                     continue
                 remote(
-                    back_out.at[step, which, n],
+                    back_out.at[which, n],
                     back.at[core, chip],
                     back_sent.at[step],
                     back_got.at[core],
@@ -588,11 +607,11 @@
     for step in range(GROUPS):
         row_copies(step).wait_recv()
         passing(step, core).start()
+        if step > 0:
+            finish(step - 1)
         passing(step, 1 - core).wait_recv()
         compute(step)
         part_copy(step).start()
-        if step > 0:
-            finish(step - 1)
     finish(GROUPS - 1)
 
     def all_back(ref, sem_sent, sem_got):
@@ -608,17 +627,19 @@
         mixture = mxu(shares, jnp.concatenate((whole, whole), axis=0), ((0,), (0,)))
         out_ref[:, lanes] = (attended[:, lanes] + mixture).astype(BF16)
 
+    sent_all(early + late)
     for copy in copies + shared:
         copy.wait_send()
     for step in range(GROUPS):
         row_copies(step).wait_send()
         passing(step, core).wait_send()
         part_copy(step).wait_send()
+        start, stop = BOUNDS[step : step + 2]
         last = 1 if step == GROUPS - 1 else 0
-        all_back(back_out.at[step, 0], back_sent.at[step], back_got.at[0]).wait_send()
-        all_back(
-            back_out.at[step, 1, pl.ds(0, span - last)], back_sent.at[step], back_got.at[0]
-        ).wait_send()
+        for which, count in enumerate((stop - start, stop - start - last)):
+            all_back(
+                back_out.at[which, pl.ds(start, count)], back_sent.at[step], back_got.at[0]
+            ).wait_send()
 
 
 def local(
@@ -645,11 +666,10 @@
     experts = chips // 2
     capacity = 2 * routes.shape[1] * half // experts
     inner = expert_gate.shape[2]
-    span = chips // GROUPS
     held = own_width // STEPS
     pairs = own_width // LANES
     chunks = width // COLUMNS
-    taken = 2 * span * capacity
+    taken = 2 * max(b - a for a, b in zip(BOUNDS, BOUNDS[1:])) * capacity
     vmem = pl.BlockSpec(memory_space=pltpu.VMEM)
     hbm = pl.BlockSpec(memory_space=pl.ANY)
     dma = pltpu.SemaphoreType.DMA
@@ -666,14 +686,14 @@
             pltpu.VMEM((width, inner), BF16),
             pltpu.VMEM((width, inner), BF16),
             pltpu.VMEM((inner, width), BF16),
-            pltpu.VMEM((pairs, 2 * HEAD, LANES), F32),
+            pltpu.VMEM((pairs, 2 * HEAD, LANES), BF16),
             pltpu.VMEM((STEPS, tokens, held), F32),
             pltpu.VMEM((STEPS, tokens, held), F32),
-            pltpu.VMEM((members, 2 * HEAD, LANES), F32),
-            pltpu.VMEM((groups, 2 * HEAD, LANES), F32),
-            pltpu.VMEM((2 * HEAD, LANES), F32),
-            pltpu.VMEM((members, HEAD, LANES), F32),
-            pltpu.VMEM((members, HEAD, LANES), F32),
+            pltpu.VMEM((members, 2 * HEAD, LANES), BF16),
+            pltpu.VMEM((groups, 2 * HEAD, LANES), BF16),
+            pltpu.VMEM((2 * HEAD, LANES), BF16),
+            pltpu.VMEM((members, HEAD, LANES), BF16),
+            pltpu.VMEM((members, HEAD, LANES), BF16),
             pltpu.VMEM((tokens, own_width), BF16),
             pltpu.VMEM((chunks, tokens, COLUMNS), F32),
             pltpu.VMEM((chunks, half, COLUMNS), F32),
@@ -681,9 +701,9 @@
             pltpu.VMEM((experts, capacity, width), BF16),
             pltpu.VMEM((2, chips, capacity, width), BF16),
             pltpu.VMEM((taken, inner), BF16),
-            pltpu.VMEM((GROUPS, 2, taken, width // 2), BF16),
-            pltpu.VMEM((GROUPS, taken, width // 2), BF16),
-            pltpu.VMEM((GROUPS, 2, span, capacity, width // 2), BF16),
+            pltpu.VMEM((2, 2 * chips * capacity, width // 2), BF16),
+            pltpu.VMEM((2 * chips * capacity, width // 2), BF16),
+            pltpu.VMEM((2, chips, capacity, width // 2), BF16),
             pltpu.VMEM((2, chips, capacity, width // 2), BF16),
             dma((STEPS, 6)),
             dma((5,)),

time: 108 us -> 96.6 us (0.89); the launches traced: 106 us -> 96.3 us
  Pallas kernels: 102 us -> 92.1 us
    pallas_call x1, Pallas kernels: 102 us -> 92.1 us  [local(): pl.pallas_call(layer_kernel, in_specs=[hbm] * 11 + [vmem] * 4, out_specs=...]
where the time goes in v4:
time: 96.6 us; the launch traced here: 96.3 us
  Pallas kernels  92.1 us (95%)
  local copies, waits for them, and re-layouts  4.23 us (4%)
    pallas_call x1, Pallas kernels, local(): pl.pallas_call(layer_kernel, in_specs=[hbm] * 11 + [vmem] * 4, out_specs=...  92.1 us

profile of v4, /device:TPU:1, one launch (start us, length us, event | category | flops | bytes accessed | tf_op | source)
XLA Modules:
  0.0 96.3 jit_solution(1722025376755438272)
XLA Ops:
  0.0 1.3 %reshape.6.gain_ref = bf16[1,1024]{1,0:T(2,128)(2,1)} reshape(bf16[1024]{0:T(1024)(128)(2,1)} %param.22) | data formatting | bytes 4096 | tf_op jit(solution)/shard_map/reshape | solution.py:737
  1.3 1.3 %reshape.7.ffn_gain_ref = bf16[1,2048]{1,0:T(2,128)(2,1)} reshape(bf16[2048]{0:T(1024)(128)(2,1)} %param.24) | data formatting | bytes 8192 | tf_op jit(solution)/shard_map/reshape | solution.py:738
  2.6 92.1 %layer.1 = bf16[64,2048]{1,0:T(8,128)(2,1)} custom-call(bf16[128,1024]{1,0:T(8,128)(2,1)} %q_ref.1, bf16[128,1024]{1,0:T(8,128)(2,1)} %k_ref.1, bf16[128,1024]{1,0:T(8,128)(2,1)} %v_ref.1, bf16[128,1024]{1,0:T(8,128)(2,1)} %r_ref.1, bf16[128,1024]{1,0:T(8,128)(2,1)} %l_ref.1, f32[128,1024]{1,0:T(8,128)} %g_ref.1, bf16[64,2048]{1,0:T(8,128)(2,1)} %stream_ref.1, ...), custom_call_target="tpu_custom_call" | custom-call | tf_op jit(solution)/shard_map/layer/pallas_call | solution.py:676
  94.7 1.7 %copy.17 = bf16[64,2048]{1,0:T(8,128)(2,1)} copy(bf16[64,2048]{1,0:T(8,128)(2,1)} %layer.1) | data formatting | bytes 524288

commit v5 on v4

--- a/solution.py
+++ b/solution.py
@@ -322,7 +322,7 @@
     variance = [mxu(packed(split(x * x)), same_head) * (1.0 / HEAD) for x in centred]
     for pair in range(pairs):
         scaled = centred[pair] * lax.rsqrt(variance[pair] + GROUP_EPS)
-        normed[:, lanes[pair]] = (scaled * gain_ref[:, lanes[pair]].astype(F32)).astype(BF16)
+        normed[:, lanes[pair]] = (scaled * gain_ref[pair : pair + 1].astype(F32)).astype(BF16)
 
 
 def slot_map(routes_ref, experts, capacity):
@@ -417,7 +417,7 @@
 ):
     group, member, core = (lax.axis_index(a) for a in ("grp", "mem", "tp"))
     members = lax.axis_size("mem")
-    chips, experts = back.shape[1], dispatched.shape[0]
+    chips, experts = back.shape[0], dispatched.shape[0]
     capacity, width = rows.shape[2:]
     half_width = width // 2
     chip = group * members + member
@@ -427,13 +427,10 @@
         return (target // members, lax.rem(target, members), which)
 
     barrier = pltpu.get_barrier_semaphore()
-    devices = 2 * chips
 
     def greet(offset, carry):
-        peer = lax.rem(2 * chip + core + offset, devices)
-        pl.semaphore_signal(
-            barrier, inc=1, device_id=at(peer // 2, lax.rem(peer, 2)), device_id_type=MESH
-        )
+        peer = at(lax.rem(chip + offset, chips), core)
+        pl.semaphore_signal(barrier, inc=1, device_id=peer, device_id_type=MESH)
         return carry
 
     held = q.shape[2]
@@ -459,7 +456,8 @@
         )
     ):
         fetches.append(pltpu.make_async_copy(source, target, fetch_sems.at[n]))
-    lax.fori_loop(1, devices, greet, 0)
+    lax.fori_loop(1, chips, greet, 0)
+    pl.semaphore_signal(barrier, inc=1, device_id=sibling, device_id_type=MESH)
     for copy in loads[: len(loads) // STEPS]:
         copy.wait()
     for copy in fetches:
@@ -477,7 +475,7 @@
         )
 
     mix(0)
-    pl.semaphore_wait(barrier, devices - 1)
+    pl.semaphore_wait(barrier, chips)
     early = member_copies(z, by_member, sent_1, got_1, 0, STEPS)
     start_all(early)
     for copy in loads[len(loads) // STEPS :]:
@@ -517,7 +515,8 @@
     scaling = lax.rsqrt(squares * (1.0 / width) + NORM_EPS)
     for n in range(chunks):
         lanes = slice(n * COLUMNS, (n + 1) * COLUMNS)
-        ffn_in = attended[:, lanes] * scaling * ffn_gain_ref[:, lanes].astype(F32)
+        gains = [ffn_gain_ref[r : r + 1] for r in range(lanes.start // LANES, lanes.stop // LANES)]
+        ffn_in = attended[:, lanes] * scaling * packed([x.astype(F32) for x in gains])
         sent_rows = mxu(picks, ffn_in.astype(BF16)).astype(BF16)
         dispatched[:, :, lanes] = sent_rows.reshape(experts, capacity, COLUMNS)
 
@@ -554,7 +553,7 @@
 
     def taken_rows(step):
         start, stop = BOUNDS[step : step + 2]
-        return slice(2 * start * capacity, 2 * stop * capacity)
+        return slice(start * capacity, stop * capacity)
 
     def part_copy(step):
         taken = taken_rows(step)
@@ -569,40 +568,40 @@
 
     def compute(step):
         start, stop = BOUNDS[step : step + 2]
-        count = 2 * (stop - start) * capacity
-        taken = rows[:, start:stop].reshape(count, width)
+        count = (stop - start) * capacity
+        taken = rows[:, start:stop].reshape(2 * count, width)
         inner = gate.shape[1]
         for begin in range(0, inner, 256):
-            lanes = slice(begin, min(begin + 256, inner))
-            gate_act = mxu(taken, gate[:, lanes])
-            up_act = mxu(taken, up[:, lanes])
-            hidden[:count, lanes] = (gate_act * jax.nn.sigmoid(gate_act) * up_act).astype(BF16)
-        for which in range(2):
-            for begin in range(0, half_width, COLUMNS):
-                columns = slice(which * half_width + begin, which * half_width + begin + COLUMNS)
-                part[which, taken_rows(step), begin : begin + COLUMNS] = mxu(
-                    hidden[:count], down[:, columns]
-                ).astype(BF16)
+            size = min(256, inner - begin)
+            lanes = slice(begin, begin + size)
+            if size == 256:
+                gate_act, up_act = mxu(taken, gate[:, lanes]), mxu(taken, up[:, lanes])
+            else:
+                both = mxu(taken, packed((gate[:, lanes], up[:, lanes])))
+                gate_act, up_act = both[:, :size], both[:, size:]
+            hidden[: 2 * count, lanes] = (gate_act * jax.nn.sigmoid(gate_act) * up_act).astype(BF16)
+        for begin in range(0, width, COLUMNS):
+            columns = slice(begin, begin + COLUMNS)
+            block = mxu(hidden[: 2 * count], down[:, columns]).astype(BF16)
+            part[0, taken_rows(step), columns] = block[:count]
+            part[1, taken_rows(step), columns] = block[count:]
 
     def finish(step):
         part_copy(step).wait_recv()
         start, stop = BOUNDS[step : step + 2]
         total = part[core, taken_rows(step)].astype(F32) + part_got[taken_rows(step)].astype(F32)
-        back_out[:, start:stop] = total.astype(BF16).reshape(2, stop - start, capacity, half_width)
+        back_out[start:stop] = total.astype(BF16).reshape(stop - start, capacity, width)
         for n in range(start, stop):
-            target = shifted(order[n], -1)
-            for turn in range(2):
-                which = 1 - core if turn == 0 else core
-                if turn == 1 and not any(order[n]):
-                    back[core, chip] = back_out[core, n]
-                    continue
-                remote(
-                    back_out.at[which, n],
-                    back.at[core, chip],
-                    back_sent.at[step],
-                    back_got.at[core],
-                    at(target, which),
-                ).start()
+            if not any(order[n]):
+                back[chip] = back_out[n]
+                continue
+            remote(
+                back_out.at[n],
+                back.at[chip],
+                back_sent.at[step],
+                back_got,
+                at(shifted(order[n], -1), core),
+            ).start()
 
     for step in range(GROUPS):
         row_copies(step).wait_recv()
@@ -617,12 +616,10 @@
     def all_back(ref, sem_sent, sem_got):
         return remote(ref, ref, sem_sent, sem_got, sibling)
 
-    for turn in range(2):
-        which = 1 - core if turn == 0 else core
-        all_back(back.at[which, pl.ds(0, chips - turn)], back_sent.at[0], back_got.at[which]).wait_recv()
+    all_back(back.at[pl.ds(0, chips - 1)], back_sent.at[0], back_got).wait_recv()
     for which in range(2):
         lanes = slice(which * half_width, (which + 1) * half_width)
-        both = back[which].reshape(experts, 2, capacity, half_width).astype(F32)
+        both = back[:, :, lanes].reshape(experts, 2, capacity, half_width).astype(F32)
         whole = (both[:, 0] + both[:, 1]).astype(BF16).reshape(experts * capacity, half_width)
         mixture = mxu(shares, jnp.concatenate((whole, whole), axis=0), ((0,), (0,)))
         out_ref[:, lanes] = (attended[:, lanes] + mixture).astype(BF16)
@@ -636,10 +633,8 @@
         part_copy(step).wait_send()
         start, stop = BOUNDS[step : step + 2]
         last = 1 if step == GROUPS - 1 else 0
-        for which, count in enumerate((stop - start, stop - start - last)):
-            all_back(
-                back_out.at[which, pl.ds(start, count)], back_sent.at[step], back_got.at[0]
-            ).wait_send()
+        count = stop - start - last
+        all_back(back_out.at[pl.ds(start, count)], back_sent.at[step], back_got).wait_send()
 
 
 def local(
@@ -701,10 +696,10 @@
             pltpu.VMEM((experts, capacity, width), BF16),
             pltpu.VMEM((2, chips, capacity, width), BF16),
             pltpu.VMEM((taken, inner), BF16),
-            pltpu.VMEM((2, 2 * chips * capacity, width // 2), BF16),
-            pltpu.VMEM((2 * chips * capacity, width // 2), BF16),
-            pltpu.VMEM((2, chips, capacity, width // 2), BF16),
-            pltpu.VMEM((2, chips, capacity, width // 2), BF16),
+            pltpu.VMEM((2, chips * capacity, width), BF16),
+            pltpu.VMEM((chips * capacity, width), BF16),
+            pltpu.VMEM((chips, capacity, width), BF16),
+            pltpu.VMEM((chips, capacity, width), BF16),
             dma((STEPS, 6)),
             dma((5,)),
             dma((members,)),
@@ -717,7 +712,7 @@
             dma((chunks,)),
         ]
         + [dma((GROUPS,))] * 7
-        + [dma((2,))],
+        + [dma],
         compiler_params=pltpu.CompilerParams(
             collective_id=0, has_side_effects=True, vmem_limit_bytes=63 * 1024 * 1024
         ),
@@ -734,8 +729,8 @@
         expert_gate,
         expert_up,
         expert_down,
-        norm_gain.reshape(1, -1),
-        ffn_gain.reshape(1, -1),
+        norm_gain.reshape(-1, LANES),
+        ffn_gain.reshape(-1, LANES),
         routes.T,
         route_weight.T,
     )

time: 96.6 us -> 91.5 us (0.947)
  local copies, waits for them, and re-layouts: 4.23 us -> 1.67 us
  Pallas kernels: 92.1 us -> 89.6 us
    reshape x2 -> x0, local copies, waits for them, and re-layouts: 2.56 us -> none  [the longest x1 1.29 us: local(): ffn_gain.reshape(1, -1)]
    pallas_call x1, Pallas kernels: 92.1 us -> 89.6 us  [local(): pl.pallas_call(layer_kernel, in_specs=[hbm] * 11 + [vmem] * 4, out_specs=...]
where the time goes in v5:
time: 91.5 us; the launch traced here: 91.3 us
  Pallas kernels  89.6 us (98%)
  local copies, waits for them, and re-layouts  1.67 us (2%)
    pallas_call x1, Pallas kernels, local(): pl.pallas_call(layer_kernel, in_specs=[hbm] * 11 + [vmem] * 4, out_specs=...  89.6 us

profile of v5, /device:TPU:1, one launch (start us, length us, event | category | flops | bytes accessed | tf_op | source)
XLA Modules:
  0.0 91.3 jit_solution(13159648053966768443)
XLA Ops:
  0.0 89.6 %layer.1 = bf16[64,2048]{1,0:T(8,128)(2,1)} custom-call(bf16[128,1024]{1,0:T(8,128)(2,1)} %q_ref.1, bf16[128,1024]{1,0:T(8,128)(2,1)} %k_ref.1, bf16[128,1024]{1,0:T(8,128)(2,1)} %v_ref.1, bf16[128,1024]{1,0:T(8,128)(2,1)} %r_ref.1, bf16[128,1024]{1,0:T(8,128)(2,1)} %l_ref.1, f32[128,1024]{1,0:T(8,128)} %g_ref.1, bf16[64,2048]{1,0:T(8,128)(2,1)} %stream_ref.1, ...), custom_call_target="tpu_custom_call" | custom-call | tf_op jit(solution)/shard_map/layer/pallas_call | solution.py:671
  89.6 1.7 %copy.17 = bf16[64,2048]{1,0:T(8,128)(2,1)} copy(bf16[64,2048]{1,0:T(8,128)(2,1)} %layer.1) | data formatting | bytes 524288

commit v6 on v5

--- a/solution.py
+++ b/solution.py
@@ -340,7 +340,7 @@
 SP_TP = ("grp", "mem", "tp")
 SP = ("grp", "mem")
 STEPS = 2
-BOUNDS = (0, 16, 32, 48, 64)
+BOUNDS = (0, 12, 28, 44, 56, 64)
 GROUPS = len(BOUNDS) - 1
 
 
@@ -396,6 +396,8 @@
     part_got,
     back_out,
     back,
+    share_rows,
+    share_of,
     in_sems,
     fetch_sems,
     sent_1,
@@ -419,19 +421,13 @@
     members = lax.axis_size("mem")
     chips, experts = back.shape[0], dispatched.shape[0]
     capacity, width = rows.shape[2:]
-    half_width = width // 2
     chip = group * members + member
     sibling = (group, member, 1 - core)
 
     def at(target, which):
-        return (target // members, lax.rem(target, members), which)
+        return (lax.div(target, members), lax.rem(target, members), which)
 
     barrier = pltpu.get_barrier_semaphore()
-
-    def greet(offset, carry):
-        peer = at(lax.rem(chip + offset, chips), core)
-        pl.semaphore_signal(barrier, inc=1, device_id=peer, device_id_type=MESH)
-        return carry
 
     held = q.shape[2]
     loads = []
@@ -456,8 +452,8 @@
         )
     ):
         fetches.append(pltpu.make_async_copy(source, target, fetch_sems.at[n]))
-    lax.fori_loop(1, chips, greet, 0)
-    pl.semaphore_signal(barrier, inc=1, device_id=sibling, device_id_type=MESH)
+    for peer in [at(lax.rem(chip + offset, chips), core) for offset in range(1, chips)] + [sibling]:
+        pl.semaphore_signal(barrier, inc=1, device_id=peer, device_id_type=MESH)
     for copy in loads[: len(loads) // STEPS]:
         copy.wait()
     for copy in fetches:
@@ -503,8 +499,7 @@
         shared[-1].start()
     kept, named = slot_map(routes_ref, experts, capacity)
     picks = kept.astype(BF16)
-    shares = kept * jnp.where(named[0], share_ref[0:1, :], share_ref[1:2, :])
-    shares = jnp.concatenate(split(shares), axis=0)
+    share_rows[...] = kept * jnp.where(named[0], share_ref[0:1, :], share_ref[1:2, :])
     squares = jnp.zeros((half, 1), F32)
     for n in range(chunks):
         lanes = slice(n * COLUMNS, (n + 1) * COLUMNS)
@@ -528,16 +523,21 @@
         place = [lax.rem(h + side + sign * o, side) for h, o in zip(here, offset)]
         return (place[0] * side + place[1]) * side + place[2]
 
-    rows[core, chips - 1] = dispatched[chip // 2]
     for n, offset in enumerate(order[:-1]):
         target = shifted(offset, 1)
         remote(
-            dispatched.at[target // 2],
+            dispatched.at[lax.div(target, 2)],
             rows.at[core, n],
             row_sent.at[sum(n >= b for b in BOUNDS[1:])],
             row_got.at[sum(n >= b for b in BOUNDS[1:])],
             at(target, core),
         ).start()
+    rows[core, chips - 1] = dispatched[chip // 2]
+    for n, offset in enumerate(order):
+        expert = lax.div(shifted(offset, 1), 2)
+        share_of[n * capacity : (n + 1) * capacity] = share_rows[
+            pl.ds(pl.multiple_of(expert * capacity, capacity), capacity)
+        ]
     for copy in fetches[2:]:
         copy.wait()
 
@@ -593,13 +593,13 @@
         back_out[start:stop] = total.astype(BF16).reshape(stop - start, capacity, width)
         for n in range(start, stop):
             if not any(order[n]):
-                back[chip] = back_out[n]
+                back[n] = back_out[n]
                 continue
             remote(
                 back_out.at[n],
-                back.at[chip],
+                back.at[n],
                 back_sent.at[step],
-                back_got,
+                back_got.at[step],
                 at(shifted(order[n], -1), core),
             ).start()
 
@@ -616,13 +616,21 @@
     def all_back(ref, sem_sent, sem_got):
         return remote(ref, ref, sem_sent, sem_got, sibling)
 
-    all_back(back.at[pl.ds(0, chips - 1)], back_sent.at[0], back_got).wait_recv()
-    for which in range(2):
-        lanes = slice(which * half_width, (which + 1) * half_width)
-        both = back[:, :, lanes].reshape(experts, 2, capacity, half_width).astype(F32)
-        whole = (both[:, 0] + both[:, 1]).astype(BF16).reshape(experts * capacity, half_width)
-        mixture = mxu(shares, jnp.concatenate((whole, whole), axis=0), ((0,), (0,)))
-        out_ref[:, lanes] = (attended[:, lanes] + mixture).astype(BF16)
+    for step in range(GROUPS):
+        start, stop = BOUNDS[step : step + 2]
+        held = back.at[pl.ds(start, min(stop, chips - 1) - start)]
+        all_back(held, back_sent.at[step], back_got.at[step]).wait_recv()
+        weights = jnp.concatenate(split(share_of[start * capacity : stop * capacity]), axis=0)
+        for begin in range(0, width, COLUMNS):
+            lanes = slice(begin, begin + COLUMNS)
+            block = back[start:stop, :, lanes].reshape((stop - start) * capacity, COLUMNS)
+            total = attended[:, lanes] + mxu(
+                weights, jnp.concatenate((block, block), axis=0), ((0,), (0,))
+            )
+            if step < GROUPS - 1:
+                attended[:, lanes] = total
+            else:
+                out_ref[:, lanes] = total.astype(BF16)
 
     sent_all(early + late)
     for copy in copies + shared:
@@ -634,7 +642,8 @@
         start, stop = BOUNDS[step : step + 2]
         last = 1 if step == GROUPS - 1 else 0
         count = stop - start - last
-        all_back(back_out.at[pl.ds(start, count)], back_sent.at[step], back_got).wait_send()
+        sent = back_out.at[pl.ds(start, count)]
+        all_back(sent, back_sent.at[step], back_got.at[step]).wait_send()
 
 
 def local(
@@ -700,6 +709,8 @@
             pltpu.VMEM((chips * capacity, width), BF16),
             pltpu.VMEM((chips, capacity, width), BF16),
             pltpu.VMEM((chips, capacity, width), BF16),
+            pltpu.VMEM((experts * capacity, half), F32),
+            pltpu.VMEM((chips * capacity, half), F32),
             dma((STEPS, 6)),
             dma((5,)),
             dma((members,)),
@@ -711,8 +722,7 @@
             dma((chunks,)),
             dma((chunks,)),
         ]
-        + [dma((GROUPS,))] * 7
-        + [dma],
+        + [dma((GROUPS,))] * 8,
         compiler_params=pltpu.CompilerParams(
             collective_id=0, has_side_effects=True, vmem_limit_bytes=63 * 1024 * 1024
         ),

time: 91.5 us -> 91.3 us (level)
  no operation moved by 1% of the time
where the time goes in v6:
time: 91.3 us; the launch traced here: 91.1 us
  Pallas kernels  89.5 us (98%)
  local copies, waits for them, and re-layouts  1.67 us (2%)
    pallas_call x1, Pallas kernels, local(): pl.pallas_call(layer_kernel, in_specs=[hbm] * 11 + [vmem] * 4, out_specs=...  89.5 us

profile of v6, /device:TPU:1, one launch (start us, length us, event | category | flops | bytes accessed | tf_op | source)
XLA Modules:
  0.0 91.1 jit_solution(10069135291412915228)
XLA Ops:
  0.0 89.5 %layer.1 = bf16[64,2048]{1,0:T(8,128)(2,1)} custom-call(bf16[128,1024]{1,0:T(8,128)(2,1)} %q_ref.1, bf16[128,1024]{1,0:T(8,128)(2,1)} %k_ref.1, bf16[128,1024]{1,0:T(8,128)(2,1)} %v_ref.1, bf16[128,1024]{1,0:T(8,128)(2,1)} %r_ref.1, bf16[128,1024]{1,0:T(8,128)(2,1)} %l_ref.1, f32[128,1024]{1,0:T(8,128)} %g_ref.1, bf16[64,2048]{1,0:T(8,128)(2,1)} %stream_ref.1, ...), custom_call_target="tpu_custom_call" | custom-call | tf_op jit(solution)/shard_map/layer/pallas_call | solution.py:680
  89.5 1.7 %copy.17 = bf16[64,2048]{1,0:T(8,128)(2,1)} copy(bf16[64,2048]{1,0:T(8,128)(2,1)} %layer.1) | data formatting | bytes 524288
